TPU v7x, 256 devices: a whole 4x4x8 slice. The times are simulated.
256 devices in a mesh: fs: 32 (over z, y), tp: 8 (over x, core).
Axes of the slice: x: 4, y: 4, z: 8, core: 2. Of those that a mesh axis runs over, the one named last changes fastest.
Arguments:
- tokens: bfloat16 [12288, 2048], P('fs', 'tp'), may hold values from -6 to 6
- norm_gain: float32 [2048], P('fs'), may hold values from 0.1 to 1.9
- gate_train: bfloat16 [8, 2048, 5632], P(None, 'fs', 'tp'), may hold values from -0.125 to 0.125
- up_train: bfloat16 [8, 2048, 5632], P(None, 'fs', 'tp'), may hold values from -0.125 to 0.125
- down_train: bfloat16 [8, 2048, 5632], P(None, 'fs', 'tp'), may hold values from -0.078125 to 0.078125
- routes: int32 [12288, 2], P('fs'), may hold values from 0 to 7, all different within a row; in each aligned block of 384 rows (0 to 383, 384 to 767, ...) at most 192 rows name the same one
- route_logits: float32 [12288, 2], P('fs'), may hold values from -6 to 6
Outputs:
- gate_weights: bfloat16 [32, 2048, 5632], P('fs', None, 'tp')
- up_weights: bfloat16 [32, 2048, 5632], P('fs', None, 'tp')
- down_weights: bfloat16 [32, 2048, 5632], P('fs', None, 'tp')
- mixed: bfloat16 [12288, 2048], P('fs', 'tp')
Inputs may be any that keep to these rules, and one draw needn't show every extreme that they name: `routes`: each row names 2 different experts; among the rows of one device no expert is named more than 192 times, and in every draw some device names some expert exactly 192 times.
All inputs are finite; a program needn't handle non-finite values.
Results may differ from a plain program's by a relative error of at most 0.014.
Values may be sent and summed in bfloat16 or wider, within the bound.
A program may use at most 128 MiB of HBM per device.

v0:
```python
import jax
import jax.numpy as jnp
from jax import lax
from jax.sharding import PartitionSpec as P

EXPERTS = 8


epsilon = 1e-06


def sent_together(arrays, axis, split_dim, concat_dim, along):
    both = jnp.concatenate(arrays, axis=along)
    result, at, done = (
        lax.all_to_all(both, axis, split_axis=split_dim, concat_axis=concat_dim, tiled=True),
        0,
        [],
    )
    for a in arrays:
        done.append(lax.slice_in_dim(result, at, at + a.shape[along], axis=along))
        at += a.shape[along]
    return tuple(done)


def slot_plan(routes, copies, capacity):
    flat_routes = routes.reshape(-1)
    experts_all = jnp.arange(EXPERTS, dtype=jnp.int32)
    onehot = (flat_routes[:, None] == experts_all[None, :]).astype(jnp.int32)
    earlier = jnp.cumsum(onehot, axis=0) - onehot
    order_rank = jnp.sum(earlier * onehot, axis=1)
    target = order_rank % copies * EXPERTS + flat_routes
    return target * capacity + order_rank // copies


def shards(tokens, norm_gain, gate_train, up_train, down_train, routes, route_logits):
    fs_count = lax.axis_size("fs")
    copies = fs_count // EXPERTS
    tok_rows = tokens.shape[0]
    capacity = tok_rows // 2 // copies
    slot_total = fs_count * capacity
    gain_rows = norm_gain[None, :, None]
    gate_low = (gate_train.astype(jnp.float32) * gain_rows).astype(jnp.bfloat16)
    up_low = (up_train.astype(jnp.float32) * gain_rows).astype(jnp.bfloat16)

    def spread(matrix):
        return jnp.tile(matrix, (copies, 1, 1))

    gate_out, up_out, down_out = sent_together(
        (spread(gate_low), spread(up_low), spread(down_train)), "fs", 0, 1, 2
    )
    slot_index = slot_plan(routes, copies, capacity)
    token_of = jnp.arange(slot_index.shape[0], dtype=jnp.int32) // routes.shape[1]
    owner = jnp.full((slot_total,), tok_rows, jnp.int32).at[slot_index].set(token_of)
    padded = jnp.concatenate([tokens, jnp.zeros((1, tokens.shape[1]), tokens.dtype)], axis=0)
    outgoing = padded[owner]
    arrived = lax.all_to_all(outgoing, "fs", split_axis=0, concat_axis=0, tiled=True)
    arrived = lax.all_gather(arrived, "tp", axis=1, tiled=True)
    arrived_float = arrived.astype(jnp.float32)
    inverse = lax.rsqrt(jnp.mean(arrived_float * arrived_float, axis=1, keepdims=True) + epsilon)
    normed = (arrived_float * inverse).astype(jnp.bfloat16)
    gate_val = jnp.dot(normed, gate_out[0], preferred_element_type=jnp.float32)
    up_val = jnp.dot(normed, up_out[0], preferred_element_type=jnp.float32)
    active = (jax.nn.silu(gate_val) * up_val).astype(jnp.bfloat16)
    down_matrix = down_out[0]
    summed = lax.psum_scatter(
        lax.dot_general(
            down_matrix, active, (((1,), (1,)), ((), ())), preferred_element_type=jnp.float32
        ).astype(jnp.bfloat16),
        "tp",
        scatter_dimension=0,
        tiled=True,
    )
    returned = lax.all_to_all(summed, "fs", split_axis=1, concat_axis=1, tiled=True)
    picked = (
        jnp.take(returned, slot_index, axis=1)
        .astype(jnp.float32)
        .reshape(returned.shape[0], tok_rows, 2)
    )
    first = jax.nn.sigmoid(route_logits[:, 0] - route_logits[:, 1])
    second = jax.nn.sigmoid(route_logits[:, 1] - route_logits[:, 0])
    mixed = picked[:, :, 0] * first[None, :] + picked[:, :, 1] * second[None, :]
    return (gate_out, up_out, down_out, mixed.T.astype(jnp.bfloat16))


def solution(mesh):
    placed = (
        P("fs", "tp"),
        P("fs"),
        P(None, "fs", "tp"),
        P(None, "fs", "tp"),
        P(None, "fs", "tp"),
        P("fs", None),
        P("fs", None),
    )
    return jax.shard_map(
        shards,
        mesh=mesh,
        in_specs=placed,
        out_specs=(P("fs", None, "tp"), P("fs", None, "tp"), P("fs", None, "tp"), P("fs", "tp")),
        check_vma=False,
    )
```

profile of v0, /device:TPU:5, one launch (start us, length us, event | category | flops | bytes accessed | tf_op | source)
XLA Modules:
  0.0 382.9 jit_solution(14041252353417813663)
XLA Ops:
  8.5 1.7 reduce-window.6
  10.8 3.4 scatter_custom_fusion
  15.2 5.4 %gather_fusion = bf16[1536,256]{1,0:T(8,128)(2,1)} fusion(bf16[385,256]{1,0:T(8,128)(2,1)S(1)} %concatenate.7, s32[2048]{0:T(1024)S(1)} %pad_clamp_fusion), kind=kCustom, calls=%fused_computation | custom fusion | bytes 1579008 | tf_op jit(solution)/shard_map/gather | solution.py:55
  20.5 11.3 %all-to-all-start.1 = ((bf16[32,48,256]{2,1,0:T(8,128)(2,1)}), bf16[32,48,256]{2,1,0:T(8,128)(2,1)}, u32[]{:S(2)}, u32[]{:S(2)}) async-start(bf16[32,48,256]{2,1,0:T(8,128)(2,1)} %bitcast.8), calls=%async_computation.1 | async-start | bytes 1572864 | tf_op jit(solution)/shard_map/all_to_all | solution.py:56
  32.8 2.0 tile.14
  34.8 2.1 tile.31
  36.9 14.5 %concatenate.6 = bf16[32,64,2112]{2,1,0:T(8,128)(2,1)} concatenate(bf16[32,64,704]{2,1,0:T(8,128)(2,1)S(1)} %bitcast.52, bf16[32,64,704]{2,1,0:T(8,128)(2,1)} %bitcast.53, bf16[32,64,704]{2,1,0:T(8,128)(2,1)} %bitcast.54), dimensions={2} | concatenate | bytes 17301504 | tf_op jit(solution)/shard_map/concatenate | solution.py:13
  51.4 1.5 all-to-all-done.1
  52.9 7.7 %all-to-all-start = ((bf16[32,64,2112]{2,1,0:T(8,128)(2,1)}), bf16[32,64,2112]{2,1,0:T(8,128)(2,1)}, u32[]{:S(2)}, u32[]{:S(2)}) async-start(bf16[32,64,2112]{2,1,0:T(8,128)(2,1)} %concatenate.6), calls=%async_computation | async-start | bytes 17825792 | tf_op jit(solution)/shard_map/all_to_all | solution.py:15
  61.4 50.9 %all-gather.2.cloned.1.call-done = bf16[1536,2048]{1,0:T(8,128)(2,1)} async-done(((bf16[1536,256]{1,0:T(8,128)(2,1)}), bf16[1536,2048]{1,0:T(8,128)(2,1)}) %all-gather.2.cloned.1.call-update) | async-done | bytes 6291472 | tf_op jit(solution)/shard_map/all_gather | solution.py:57
  112.4 4.2 %fusion = f32[1536]{0:T(1024)S(1)} fusion(bf16[1536,2048]{1,0:T(8,128)(2,1)} %all-gather.2.cloned.1.call-done), kind=kLoop, calls=%fused_computation.5 | loop fusion | flops 9435648 | bytes 6297600 | tf_op jit(solution)/shard_map/reduce_sum | solution.py:59
  116.6 141.5 %all-to-all-done = bf16[32,64,2112]{2,1,0:T(8,128)(2,1)} async-done(((bf16[32,64,2112]{2,1,0:T(8,128)(2,1)}), bf16[32,64,2112]{2,1,0:T(8,128)(2,1)}, u32[]{:S(2)}, u32[]{:S(2)}) %all-to-all-start) | async-done | bytes 8650784 | tf_op jit(solution)/shard_map/all_to_all | solution.py:15
  258.1 8.8 %fusion.3 = f32[1536,704]{0,1:T(8,128)S(1)} fusion(bf16[1536,2048]{1,0:T(8,128)(2,1)} %all-gather.2.cloned.1.call-done, f32[1536]{0:T(1024)S(1)} %add_rsqrt_fusion, bf16[1,2048,2112]{2,1,0:T(8,128)(2,1)} %bitcast.3), kind=kOutput, calls=%fused_computation.10 | convolution fusion | flops 4438622208 | bytes 13768704 | tf_op jit(solution)/shard_map/dot_general | solution.py:61
  266.9 8.3 %multiply_convert_fusion = bf16[1536,704]{0,1:T(8,128)(2,1)S(1)} fusion(f32[1536,704]{0,1:T(8,128)S(1)} %fusion.3, bf16[1536,2048]{1,0:T(8,128)(2,1)S(1)} %bitcast.56, f32[1536]{0:T(1024)S(1)} %add_rsqrt_fusion, bf16[1,2048,2112]{2,1,0:T(8,128)(2,1)} %bitcast.3), kind=kOutput, calls=%fused_computation.8 | convolution fusion | flops 4445110272 | bytes 15931392 | tf_op jit(solution)/shard_map/dot_general | solution.py:62
  275.2 8.9 %convolution_convert_fusion = bf16[2048,1536]{1,0:T(8,128)(2,1)} fusion(bf16[1536,704]{0,1:T(8,128)(2,1)S(1)} %multiply_convert_fusion, bf16[1,2048,2112]{2,1,0:T(8,128)(2,1)} %bitcast.3), kind=kOutput, calls=%fused_computation.7 | convolution fusion | flops 4432330752 | bytes 11599872 | tf_op jit(solution)/shard_map/dot_general | solution.py:66
  284.1 54.1 %reduce-scatter.2.cloned.1.call-done = bf16[256,1536]{1,0:T(8,128)(2,1)} async-done(((bf16[2048,1536]{1,0:T(8,128)(2,1)}), bf16[256,1536]{1,0:T(8,128)(2,1)}) %reduce-scatter.2.cloned.1.call-update) | async-done | bytes 786448 | tf_op jit(solution)/shard_map/reduce_scatter | solution.py:65
  338.2 2.3 copy.47
  340.4 9.8 %all-to-all-start.2 = ((bf16[256,32,48]{0,2,1:T(8,128)(2,1)}), bf16[256,32,48]{0,2,1:T(8,128)(2,1)S(1)}, u32[]{:S(2)}, u32[]{:S(2)}) async-start(bf16[256,32,48]{0,2,1:T(8,128)(2,1)} %bitcast.12), calls=%async_computation.3 | async-start | bytes 1572864 | tf_op jit(solution)/shard_map/all_to_all | solution.py:73
  350.6 6.8 %fusion.31 = (bf16[1,2048,704]{2,1,0:T(8,128)(2,1)}, bf16[1,2048,704]{2,1,0:T(8,128)(2,1)}, bf16[1,2048,704]{2,1,0:T(8,128)(2,1)}) fusion(bf16[1,2048,2112]{2,1,0:T(8,128)(2,1)} %bitcast.3), kind=kLoop, calls=%fused_computation.67 | loop fusion | bytes 17301504 | tf_op jit(solution)/shard_map/slice | solution.py:20
  357.5 4.6 %copy.49 = bf16[1,2048,704]{1,2,0:T(8,128)(2,1)} copy(bf16[1,2048,704]{2,1,0:T(8,128)(2,1)} %get-tuple-element.16) | data formatting | bytes 5767168
  362.0 4.6 %copy.50 = bf16[1,2048,704]{1,2,0:T(8,128)(2,1)} copy(bf16[1,2048,704]{2,1,0:T(8,128)(2,1)} %get-tuple-element.15) | data formatting | bytes 5767168
  366.6 4.6 %copy.51 = bf16[1,2048,704]{1,2,0:T(8,128)(2,1)} copy(bf16[1,2048,704]{2,1,0:T(8,128)(2,1)} %get-tuple-element.14) | data formatting | bytes 5767168
  371.1 1.1 all-to-all-done.2
  372.2 2.6 gather_fusion.1
  (47 shorter events, 6.0 us)
Async XLA Ops:
  15.1 16.7 %copy-start = (bf16[8,64,704]{2,1,0:T(8,128)(2,1)S(1)}, bf16[8,64,704]{2,1,0:T(8,128)(2,1)}, u32[]{:S(2)}) copy-start(bf16[8,64,704]{2,1,0:T(8,128)(2,1)} %param.10) | copy-start | bytes 2162692
  15.2 16.7 %copy-start.1 = (bf16[8,64,704]{2,1,0:T(8,128)(2,1)S(1)}, bf16[8,64,704]{2,1,0:T(8,128)(2,1)}, u32[]{:S(2)}) copy-start(bf16[8,64,704]{2,1,0:T(8,128)(2,1)} %param.9) | copy-start | bytes 2162692
  15.2 16.7 %copy-start.5 = (f32[64]{0:T(128)S(1)}, f32[64]{0:T(128)}, u32[]{:S(2)}) copy-start(f32[64]{0:T(128)} %param.8) | copy-start | bytes 772
  20.5 32.4 %all-to-all-start.1 = ((bf16[32,48,256]{2,1,0:T(8,128)(2,1)}), bf16[32,48,256]{2,1,0:T(8,128)(2,1)}, u32[]{:S(2)}, u32[]{:S(2)}) async-start(bf16[32,48,256]{2,1,0:T(8,128)(2,1)} %bitcast.8), calls=%async_computation.1 | async-start | bytes 1572864 | tf_op jit(solution)/shard_map/all_to_all | solution.py:56
  32.4 2.4 copy-start.2
  52.9 205.2 %all-to-all-start = ((bf16[32,64,2112]{2,1,0:T(8,128)(2,1)}), bf16[32,64,2112]{2,1,0:T(8,128)(2,1)}, u32[]{:S(2)}, u32[]{:S(2)}) async-start(bf16[32,64,2112]{2,1,0:T(8,128)(2,1)} %concatenate.6), calls=%async_computation | async-start | bytes 17825792 | tf_op jit(solution)/shard_map/all_to_all | solution.py:15
  60.7 51.7 %all-gather.2.cloned.1.call-start = ((), (), s32[]{:S(2)}) async-start(), calls=%async_computation.4 | async-start | bytes 7077888 | tf_op jit(solution)/shard_map/all_gather | solution.py:57
  61.4 276.8 %reduce-scatter.2.cloned.1.call-start = ((), (), s32[]{:S(2)}) async-start(), calls=%async_computation.5 | async-start | bytes 7077888 | tf_op jit(solution)/shard_map/reduce_scatter | solution.py:65
  112.4 154.5 %slice-start = ((s8[6291456]{0:T(1024)(128)(4,1)}), s8[2097152]{0:T(1024)(128)(4,1)S(1)}, s32[]{:S(2)}) async-start(s8[6291456]{0:T(1024)(128)(4,1)} %bitcast.55), calls=%async_computation.6 | async-start | bytes 4194304
  258.1 8.8 %slice-start.1 = ((s8[6291456]{0:T(1024)(128)(4,1)}), s8[4194304]{0:T(1024)(128)(4,1)S(1)}, s32[]{:S(2)}) async-start(s8[6291456]{0:T(1024)(128)(4,1)} %bitcast.55), calls=%async_computation.7 | async-start | bytes 8388608
  284.1 66.5 %copy-start.4 = (f32[384,2]{0,1:T(2,128)S(1)}, f32[384,2]{0,1:T(2,128)}, u32[]{:S(2)}) copy-start(f32[384,2]{0,1:T(2,128)} %param.13) | copy-start | bytes 9220
  284.1 66.5 %copy-start.3 = (s32[384,2]{0,1:T(2,128)S(1)}, s32[384,2]{0,1:T(2,128)}, u32[]{:S(2)}) copy-start(s32[384,2]{0,1:T(2,128)} %param.12) | copy-start | bytes 9220
  340.4 31.8 %all-to-all-start.2 = ((bf16[256,32,48]{0,2,1:T(8,128)(2,1)}), bf16[256,32,48]{0,2,1:T(8,128)(2,1)S(1)}, u32[]{:S(2)}, u32[]{:S(2)}) async-start(bf16[256,32,48]{0,2,1:T(8,128)(2,1)} %bitcast.12), calls=%async_computation.3 | async-start | bytes 1572864 | tf_op jit(solution)/shard_map/all_to_all | solution.py:73
Sparse Core Ops, SparseCore 0:
  63.3 49.0 all-gather.1
  284.2 53.8 reduce-scatter.1
where the time goes:
time: 385 us; the launch traced here: 383 us
  waiting for transfers between devices  250 us (65%)
  local copies, waits for them, and re-layouts  56.1 us (15%)
  starting transfers between devices  28.9 us (8%)
  matrix products  25.9 us (7%)
  between operations  14.3 us (4%)
  other arithmetic  7.84 us (2%)
    all_to_all x1, waiting for transfers between devices, sent_together(): lax.all_to_all(both, axis, split_axis=split_dim, concat_axis=concat_dim,...  141 us
    reduce_scatter x1, waiting for transfers between devices, shards(): lax.psum_scatter(lax.dot_general(down_matrix, active, (((1,), (1,)), ((),...  54.1 us
    all_gather x1, waiting for transfers between devices, shards(): arrived = lax.all_gather(arrived, 'tp', axis=1, tiled=True)  50.9 us
    unnamed x20, local copies, waits for them, and re-layouts  14.6 us
    concatenate x1, local copies, waits for them, and re-layouts, sent_together(): both = jnp.concatenate(arrays, axis=along)  14.5 us
    all_to_all x1, starting transfers between devices, shards(): lax.all_to_all(outgoing, 'fs', split_axis=0, concat_axis=0, tiled=True)  11.3 us
    all_to_all x1, starting transfers between devices, shards(): lax.all_to_all(summed, 'fs', split_axis=1, concat_axis=1, tiled=True)  9.81 us
    dot_general x1, matrix products, shards(): lax.dot_general(down_matrix, active, (((1,), (1,)), ((), ())), preferred_...  8.9 us
  transfers between devices with their start and end apart: 5, of which 5 were waited for; matrix products, arithmetic and copies ran while one was open for 12% of the time, Pallas kernels for 0%

commit v1 on v0

v1 whole, which is shorter than its diff:
```python
import functools

import jax
import jax.numpy as jnp
from jax import lax
from jax.experimental import pallas as pl
from jax.experimental.pallas import tpu as pltpu
from jax.sharding import PartitionSpec as P

EXPERTS = 8
epsilon = 1e-06
MESH = pl.DeviceIdType.MESH
NZ, NY = 8, 4
PARTS = ((0, 384), (384, 320))


def weights_kernel(g_ref, u_ref, d_ref, og, ou, od, y0, y1, away, ysend, yrecv, zsend, zrecv):
    fs = lax.axis_index("fs")
    z, y = fs // NY, lax.rem(fs, NY)
    parity = lax.rem(z, 2)
    sources, outs, ybufs = (g_ref, u_ref, d_ref), (og, ou, od), (y0, y1)
    rows = g_ref.shape[2]

    def zat(step):
        return lax.rem(z + step + NZ, NZ)

    def yat(step):
        return lax.rem(y + step + NY, NY)

    def device(dz, dy):
        return {"fs": zat(dz) * NY + yat(dy)}

    barrier = pltpu.get_barrier_semaphore()
    partners = [(0, 1), (0, 2), (0, 3), (1, 0), (-1, 0), (2, 0), (-2, 0)]
    for dz, dy in partners:
        pl.semaphore_signal(barrier, inc=1, device_id=device(dz, dy), device_id_type=MESH)
    pl.semaphore_wait(barrier, len(partners))

    units = [(m, h) for m in range(3) for h in range(2)]

    def ycopy(u, dy, to_row):
        m, h = units[u]
        lo, n = PARTS[h]
        return pltpu.make_async_remote_copy(
            src_ref=sources[m].at[:, yat(dy), :, pl.ds(lo, n)],
            dst_ref=ybufs[h].at[m, :, pl.ds(to_row * rows, rows), :],
            send_sem=ysend.at[u * 3 + dy - 1],
            recv_sem=yrecv.at[u * 3 + dy - 1],
            device_id=device(0, dy),
            device_id_type=MESH,
        )

    def zcopy(u, kind, sign, arriving=False):
        m, h = units[u]
        lo, n = PARTS[h]
        out = outs[m]
        near = {"a": 1, "b": 2, "c": 2, "d": 2}[kind]
        hops = {"a": 0, "b": 0, "c": 1, "d": 2}[kind]
        block = zat(-sign * hops)
        if arriving:
            block = zat(-sign * (hops + near))
        if kind == "d":
            half = n // 2
            lo, n = (lo, half) if sign > 0 else (lo + half, half)
        place = out.at[block, pl.ds(lo, n), :]
        source = away.at[m, pl.ds(lo, n), :] if kind == "a" else place
        at = u * 8 + "abcd".index(kind) * 2 + (0 if sign > 0 else 1)
        return pltpu.make_async_remote_copy(
            src_ref=source,
            dst_ref=place,
            send_sem=zsend.at[at],
            recv_sem=zrecv.at[at],
            device_id=device(sign * near, 0),
            device_id_type=MESH,
        )

    for u in range(6):
        for dy in (1, 3, 2):
            ycopy(u, dy, y).start()
    for m in range(3):
        for h, (lo, n) in enumerate(PARTS):
            ybufs[h][m, :, pl.ds(y * rows, rows), :] = sources[m][:, y, :, lo : lo + n]

    def turn(u):
        m, h = units[u]
        lo, n = PARTS[h]
        for dy in (1, 3, 2):
            ycopy(u, dy, yat(-dy)).wait_recv()
        away[m, pl.ds(lo, n), :] = ybufs[h][m, 1 - parity].T
        outs[m][z, pl.ds(lo, n), :] = ybufs[h][m, parity].T

    def first(u):
        turn(u)
        for kind in "ab":
            for sign in (1, -1):
                zcopy(u, kind, sign).start()

    def second(u):
        for kind, after in (("a", "c"), ("b", "d")):
            for sign in (1, -1):
                zcopy(u, kind, sign, True).wait_recv()
                zcopy(u, after, sign).start()

    first(0)
    for u in range(6):
        if u < 5:
            first(u + 1)
        second(u)
    for u in range(6):
        for kind in "cd":
            for sign in (1, -1):
                zcopy(u, kind, sign, True).wait_recv()
    for u in range(6):
        for dy in (1, 3, 2):
            ycopy(u, dy, y).wait_send()
        for kind in "abcd":
            for sign in (1, -1):
                zcopy(u, kind, sign).wait_send()


def handed_over(gate, up, down):
    _, rows, width = gate.shape
    split = [w.reshape(2, NY, rows, width) for w in (gate, up, down)]
    out = jax.ShapeDtypeStruct((NZ, width, NY * rows), jnp.bfloat16)
    dma = pltpu.SemaphoreType.DMA
    return pl.pallas_call(
        weights_kernel,
        out_shape=(out, out, out),
        in_specs=[pl.BlockSpec(memory_space=pltpu.VMEM)] * 3,
        out_specs=(pl.BlockSpec(memory_space=pltpu.VMEM),) * 3,
        scratch_shapes=[
            pltpu.VMEM((3, 2, NY * rows, PARTS[0][1]), jnp.bfloat16),
            pltpu.VMEM((3, 2, NY * rows, PARTS[1][1]), jnp.bfloat16),
            pltpu.VMEM((3, width, NY * rows), jnp.bfloat16),
            dma((18,)),
            dma((18,)),
            dma((48,)),
            dma((48,)),
        ],
        compiler_params=pltpu.CompilerParams(
            collective_id=0, has_side_effects=True, vmem_limit_bytes=40 * 1024 * 1024
        ),
        cost_estimate=pl.CostEstimate(flops=10**11, bytes_accessed=10**7, transcendentals=0),
    )(*split)


def slot_plan(routes, most):
    experts_all = jnp.arange(EXPERTS, dtype=jnp.int32)
    named = (routes.T[:, None, :] == experts_all[None, :, None]).astype(jnp.bfloat16)
    tokens = routes.shape[0]
    places = jnp.arange(tokens)
    before = (places[:, None] < places[None, :]).astype(jnp.bfloat16)
    rank = jnp.dot(named.reshape(-1, tokens), before, preferred_element_type=jnp.float32)
    rank = rank.reshape(named.shape)
    count = jnp.sum(named[0].astype(jnp.float32), axis=1)
    rank = rank + jnp.stack([jnp.zeros_like(count), count])[:, :, None]
    slot = rank + most * experts_all[None, :, None].astype(jnp.float32)
    return jnp.sum(jnp.where(named > 0, slot, 0.0), axis=1).astype(jnp.int32)


def shards(tokens, norm_gain, gate_train, up_train, down_train, routes, route_logits):
    fs_count = lax.axis_size("fs")
    groups = [list(range(at, at + EXPERTS)) for at in range(0, fs_count, EXPERTS)]
    tok_rows, features = tokens.shape
    most = tok_rows // 2
    gain_rows = norm_gain[None, :, None]
    gate_low = (gate_train.astype(jnp.float32) * gain_rows).astype(jnp.bfloat16)
    up_low = (up_train.astype(jnp.float32) * gain_rows).astype(jnp.bfloat16)

    slots = slot_plan(routes, most)
    slot_ids = jnp.arange(EXPERTS * most, dtype=jnp.int32)
    chosen = [(slots[k][None, :] == slot_ids[:, None]).astype(jnp.bfloat16) for k in range(2)]
    outgoing = jnp.dot(chosen[0] + chosen[1], tokens, preferred_element_type=jnp.float32)
    outgoing = outgoing.astype(jnp.bfloat16).reshape(EXPERTS, most, features)
    arrived = lax.all_to_all(
        outgoing, "fs", split_axis=0, concat_axis=0, tiled=True, axis_index_groups=groups
    )
    arrived = arrived.reshape(EXPERTS * most, features)
    arrived, gate_low, up_low, down_low = lax.optimization_barrier(
        (arrived, gate_low, up_low, down_train)
    )
    handed = handed_over(gate_low, up_low, down_low)
    gate_out, up_out, down_out = (
        w.transpose(0, 2, 1).reshape(1, -1, gate_train.shape[2]) for w in handed
    )
    arrived = lax.all_gather(arrived, "tp", axis=1, tiled=True)
    arrived_float = arrived.astype(jnp.float32)
    inverse = lax.rsqrt(jnp.mean(arrived_float * arrived_float, axis=1, keepdims=True) + epsilon)
    normed = (arrived_float * inverse).astype(jnp.bfloat16)
    gate_val = jnp.dot(normed, gate_out[0], preferred_element_type=jnp.float32)
    up_val = jnp.dot(normed, up_out[0], preferred_element_type=jnp.float32)
    active = (jax.nn.silu(gate_val) * up_val).astype(jnp.bfloat16)
    summed = lax.psum_scatter(
        lax.dot_general(
            active, down_out[0], (((1,), (1,)), ((), ())), preferred_element_type=jnp.float32
        ).astype(jnp.bfloat16),
        "tp",
        scatter_dimension=1,
        tiled=True,
    )
    returned = lax.all_to_all(
        summed.reshape(EXPERTS, most, features),
        "fs",
        split_axis=0,
        concat_axis=0,
        tiled=True,
        axis_index_groups=groups,
    ).reshape(EXPERTS * most, features)
    picked = [
        lax.dot_general(
            c, returned, (((0,), (0,)), ((), ())), preferred_element_type=jnp.float32
        )
        for c in chosen
    ]
    first = jax.nn.sigmoid(route_logits[:, 0] - route_logits[:, 1])
    second = jax.nn.sigmoid(route_logits[:, 1] - route_logits[:, 0])
    mixed = picked[0] * first[:, None] + picked[1] * second[:, None]
    return (gate_out, up_out, down_out, mixed.astype(jnp.bfloat16))


def solution(mesh):
    placed = (
        P("fs", "tp"),
        P("fs"),
        P(None, "fs", "tp"),
        P(None, "fs", "tp"),
        P(None, "fs", "tp"),
        P("fs", None),
        P("fs", None),
    )
    return jax.shard_map(
        shards,
        mesh=mesh,
        in_specs=placed,
        out_specs=(P("fs", None, "tp"), P("fs", None, "tp"), P("fs", None, "tp"), P("fs", "tp")),
        check_vma=False,
    )
```

time: 385 us -> 319 us (0.83)
  waiting for transfers between devices: 250 us -> 72.6 us
  Pallas kernels: 0 us -> 135 us
  starting transfers between devices: 28.9 us -> 10.6 us
  local copies, waits for them, and re-layouts: 56.1 us -> 42.6 us
  matrix products: 25.9 us -> 34.5 us
    pallas_call x0 -> x1, Pallas kernels: none -> 135 us  [handed_over(): pl.pallas_call(weights_kernel, out_shape=(out, out, out), in_specs=[pl.Bl...]
    all_to_all x3 -> x2, waiting for transfers between devices: 144 us -> 9.84 us  [the longest x1 9.84 us: shards(): lax.all_to_all(outgoing, 'fs', split_axis=0, concat_axis=0, tiled=True, a...]
    all_gather x1, waiting for transfers between devices: 50.9 us -> 0.01 us  [shards(): arrived = lax.all_gather(arrived, 'tp', axis=1, tiled=True)]
    all_to_all x3 -> x2, starting transfers between devices: 28.9 us -> 10.5 us  [the longest x1 5.55 us: shards(): lax.all_to_all(outgoing, 'fs', split_axis=0, concat_axis=0, tiled=True, a...]
    reshape x1 -> x3, local copies, waits for them, and re-layouts: 0.15 us -> 16.7 us  [shards(): w.transpose(0, 2, 1).reshape(1, -1, gate_train.shape[2])]
    concatenate x2 -> x0, local copies, waits for them, and re-layouts: 15.4 us -> none  [the longest x1 14.5 us: sent_together(): both = jnp.concatenate(arrays, axis=along)]
    transpose x0 -> x3, local copies, waits for them, and re-layouts: none -> 13.2 us  [shards(): w.transpose(0, 2, 1).reshape(1, -1, gate_train.shape[2])]
    dot_general x2 -> x5, matrix products: 17.2 us -> 26.2 us  [the longest x1 19.1 us: shards(): lax.dot_general(active, down_out[0], (((1,), (1,)), ((), ())), preferred_...]
  transfers between devices with their start and end apart: 5 -> 4, of which waited for: 5 -> 2; matrix products, arithmetic and copies ran while one was open for 12% -> 12% of each run, Pallas kernels for 0% -> 43%
where the time goes in v1:
time: 319 us; the launch traced here: 317 us
  Pallas kernels  135 us (42%)
  waiting for transfers between devices  72.6 us (23%)
  local copies, waits for them, and re-layouts  42.6 us (13%)
  matrix products  34.5 us (11%)
  between operations  14.2 us (4%)
  starting transfers between devices  10.6 us (3%)
  other arithmetic  6.85 us (2%)
    pallas_call x1, Pallas kernels, handed_over(): pl.pallas_call(weights_kernel, out_shape=(out, out, out), in_specs=[pl.Bl...  135 us
    reduce_scatter x1, waiting for transfers between devices, shards(): lax.psum_scatter(lax.dot_general(active, down_out[0], (((1,), (1,)), ((),...  62.7 us
    dot_general x1, matrix products, shards(): lax.dot_general(active, down_out[0], (((1,), (1,)), ((), ())), preferred_...  19.1 us
    reshape x3, local copies, waits for them, and re-layouts, shards(): w.transpose(0, 2, 1).reshape(1, -1, gate_train.shape[2])  16.7 us
    transpose x3, local copies, waits for them, and re-layouts, shards(): w.transpose(0, 2, 1).reshape(1, -1, gate_train.shape[2])  13.2 us
    all_to_all x1, waiting for transfers between devices, shards(): lax.all_to_all(outgoing, 'fs', split_axis=0, concat_axis=0, tiled=True, a...  9.84 us
    dot_general x1, matrix products, shards(): gate_val = jnp.dot(normed, gate_out[0], preferred_element_type=jnp.float32)  8.34 us
    unnamed x32, local copies, waits for them, and re-layouts  6.42 us
  transfers between devices with their start and end apart: 4, of which 2 were waited for; matrix products, arithmetic and copies ran while one was open for 12% of the time, Pallas kernels for 43%

profile of v1, /device:TPU:5, one launch (start us, length us, event | category | flops | bytes accessed | tf_op | source)
XLA Modules:
  0.0 316.6 jit_solution(12280452666625783121)
XLA Ops:
  9.7 1.6 convolution_convert_fusion.1
  11.3 5.5 %all-to-all-start = ((bf16[8,192,256]{2,1,0:T(8,128)(2,1)}), bf16[8,192,256]{2,1,0:T(8,128)(2,1)S(1)}, u32[]{:S(2)}, u32[]{:S(2)}) async-start(bf16[8,192,256]{2,1,0:T(8,128)(2,1)} %bitcast.3), calls=%async_computation | async-start | bytes 1572864 | tf_op jit(solution)/shard_map/all_to_all | solution.py:175
  16.9 1.6 multiply_convert_fusion.1
  18.5 9.8 %all-to-all-done = bf16[8,192,256]{2,1,0:T(8,128)(2,1)S(1)} async-done(((bf16[8,192,256]{2,1,0:T(8,128)(2,1)}), bf16[8,192,256]{2,1,0:T(8,128)(2,1)S(1)}, u32[]{:S(2)}, u32[]{:S(2)}) %all-to-all-start) | async-done | bytes 786464 | tf_op jit(solution)/shard_map/all_to_all | solution.py:175
  29.3 1.1 copy-done.3
  30.5 1.1 copy-done.4
  31.6 1.1 copy-done.5
  32.7 135.2 %shard_map.102 = (bf16[8,704,256]{2,1,0:T(8,128)(2,1)S(1)}, bf16[8,704,256]{2,1,0:T(8,128)(2,1)S(1)}, bf16[8,704,256]{2,1,0:T(8,128)(2,1)S(1)}) custom-call(bf16[2,4,64,704]{3,2,1,0:T(8,128)(2,1)S(1)} %bitcast.40, bf16[2,4,64,704]{3,2,1,0:T(8,128)(2,1)S(1)} %bitcast.39, bf16[2,4,64,704]{3,2,1,0:T(8,128)(2,1)S(1)} %bitcast.41), custom_call_target="tpu_custom_call" | custom-call | flops 99999997952 | bytes 10000000 | tf_op jit(solution)/shard_map/pallas_call | solution.py:126
  168.0 2.2 copy.17
  171.4 2.0 copy.18
  173.4 2.0 copy.19
  175.4 4.2 %fusion = f32[1536]{0:T(1024)S(1)} fusion(bf16[1536,2048]{1,0:T(8,128)(2,1)} %all-gather.2.cloned.1.call-done), kind=kLoop, calls=%fused_computation.2 | loop fusion | flops 9435648 | bytes 6297600 | tf_op jit(solution)/shard_map/reduce_sum | solution.py:188
  180.0 8.3 %fusion.3 = f32[1536,704]{0,1:T(8,128)} fusion(bf16[2048,704]{0,1:T(8,128)(2,1)} %bitcast.45, bf16[1536,2048]{1,0:T(8,128)(2,1)S(1)} %copy-done.6, f32[1536]{0:T(1024)S(1)} %add_rsqrt_fusion), kind=kOutput, calls=%fused_computation.7 | convolution fusion | flops 4438622208 | bytes 13506560 | tf_op jit(solution)/shard_map/dot_general | solution.py:190
  188.3 19.1 %convolution_convert_fusion = bf16[1536,2048]{1,0:T(8,128)(2,1)} fusion(bf16[2048,704]{0,1:T(8,128)(2,1)} %bitcast.44, f32[1536,704]{0,1:T(8,128)} %fusion.3, bf16[2048,704]{0,1:T(8,128)(2,1)} %bitcast.43, bf16[1536,2048]{1,0:T(8,128)(2,1)} %all-gather.2.cloned.1.call-done, f32[1536]{0:T(1024)S(1)} %add_rsqrt_fusion), kind=kOutput, calls=%fused_computation.4 | convolution fusion | flops 8877441024 | bytes 22681600 | tf_op jit(solution)/shard_map/dot_general | solution.py:194
  207.5 62.7 %reduce-scatter.2.cloned.1.call-done = bf16[1536,256]{1,0:T(8,128)(2,1)} async-done(((bf16[1536,2048]{1,0:T(8,128)(2,1)}), bf16[1536,256]{1,0:T(8,128)(2,1)}) %reduce-scatter.2.cloned.1.call-update) | async-done | bytes 786448 | tf_op jit(solution)/shard_map/reduce_scatter | solution.py:193
  270.2 5.0 %all-to-all-start.1 = ((bf16[8,192,256]{2,1,0:T(8,128)(2,1)}), bf16[8,192,256]{2,1,0:T(8,128)(2,1)}, u32[]{:S(2)}, u32[]{:S(2)}) async-start(bf16[8,192,256]{2,1,0:T(8,128)(2,1)} %bitcast.46), calls=%async_computation.2 | async-start | bytes 1572864 | tf_op jit(solution)/shard_map/all_to_all | solution.py:201
  275.2 5.0 %copy.11 = bf16[8,256,704]{1,0,2:T(8,128)(2,1)} copy(bf16[8,256,704]{1,2,0:T(8,128)(2,1)} %bitcast.38) | data formatting | bytes 5767168 | tf_op jit(solution)/shard_map/transpose | solution.py:184
  280.2 5.6 %reshape.72 = bf16[1,2048,704]{1,2,0:T(8,128)(2,1)} reshape(bf16[8,256,704]{1,0,2:T(8,128)(2,1)} %copy.11) | data formatting | bytes 5767168 | tf_op jit(solution)/shard_map/reshape | solution.py:184
  285.8 5.0 %copy.12 = bf16[8,256,704]{1,0,2:T(8,128)(2,1)} copy(bf16[8,256,704]{1,2,0:T(8,128)(2,1)} %bitcast.36) | data formatting | bytes 5767168 | tf_op jit(solution)/shard_map/transpose | solution.py:184
  290.8 5.6 %reshape.73 = bf16[1,2048,704]{1,2,0:T(8,128)(2,1)} reshape(bf16[8,256,704]{1,0,2:T(8,128)(2,1)} %copy.12) | data formatting | bytes 5767168 | tf_op jit(solution)/shard_map/reshape | solution.py:184
  296.4 3.2 %copy.13 = bf16[8,256,704]{1,0,2:T(8,128)(2,1)} copy(bf16[8,256,704]{1,2,0:T(8,128)(2,1)S(1)} %bitcast.34) | data formatting | bytes 5767168 | tf_op jit(solution)/shard_map/transpose | solution.py:184
  299.6 5.6 %reshape.74 = bf16[1,2048,704]{1,2,0:T(8,128)(2,1)} reshape(bf16[8,256,704]{1,0,2:T(8,128)(2,1)} %copy.13) | data formatting | bytes 5767168 | tf_op jit(solution)/shard_map/reshape | solution.py:184
  305.2 1.9 fusion.13
  307.1 2.6 fusion.21
  (44 shorter events, 5.1 us)
Async XLA Ops:
  7.2 2.6 copy-start
  7.2 9.7 %copy-start.8 = (bf16[8,64,704]{2,1,0:T(8,128)(2,1)S(1)}, bf16[8,64,704]{2,1,0:T(8,128)(2,1)}, u32[]{:S(2)}) copy-start(bf16[8,64,704]{2,1,0:T(8,128)(2,1)} %param.10) | copy-start | bytes 2162692
  7.2 9.7 %copy-start.15 = (f32[64]{0:T(128)S(1)}, f32[64]{0:T(128)}, u32[]{:S(2)}) copy-start(f32[64]{0:T(128)} %param.8) | copy-start | bytes 772
  7.2 9.7 %copy-start.9 = (bf16[8,64,704]{2,1,0:T(8,128)(2,1)S(1)}, bf16[8,64,704]{2,1,0:T(8,128)(2,1)}, u32[]{:S(2)}) copy-start(bf16[8,64,704]{2,1,0:T(8,128)(2,1)} %param.9) | copy-start | bytes 2162692
  9.1 0.6 copy-start.11
  9.2 2.1 copy-start.13
  11.3 17.1 %all-to-all-start = ((bf16[8,192,256]{2,1,0:T(8,128)(2,1)}), bf16[8,192,256]{2,1,0:T(8,128)(2,1)S(1)}, u32[]{:S(2)}, u32[]{:S(2)}) async-start(bf16[8,192,256]{2,1,0:T(8,128)(2,1)} %bitcast.3), calls=%async_computation | async-start | bytes 1572864 | tf_op jit(solution)/shard_map/all_to_all | solution.py:175
  16.8 158.6 %all-gather.2.cloned.1.call-start = ((), (), s32[]{:S(2)}) async-start(), calls=%async_computation.3 | async-start | bytes 7077888 | tf_op jit(solution)/shard_map/all_gather | solution.py:186
  28.4 0.9 copy-start.7
  29.3 240.9 %reduce-scatter.2.cloned.1.call-start = ((), (), s32[]{:S(2)}) async-start(), calls=%async_computation.4 | async-start | bytes 7077888 | tf_op jit(solution)/shard_map/reduce_scatter | solution.py:193
  29.3 1.1 copy-start.3
  30.5 1.1 copy-start.4
  31.6 1.1 copy-start.5
  168.0 2.4 copy-start.2
  168.0 3.4 %copy-start.1 = (bf16[8,704,256]{2,1,0:T(8,128)(2,1)}, bf16[8,704,256]{2,1,0:T(8,128)(2,1)S(1)}, u32[]{:S(2)}) copy-start(bf16[8,704,256]{2,1,0:T(8,128)(2,1)S(1)} %get-tuple-element.15) | copy-start | bytes 8650756
  175.4 4.6 %copy-start.6 = (bf16[1536,2048]{1,0:T(8,128)(2,1)S(1)}, bf16[1536,2048]{1,0:T(8,128)(2,1)}, u32[]{:S(2)}) copy-start(bf16[1536,2048]{1,0:T(8,128)(2,1)} %all-gather.2.cloned.1.call-done) | copy-start | bytes 18874372
  207.4 67.7 %copy-start.10 = (f32[384,2]{0,1:T(2,128)S(1)}, f32[384,2]{0,1:T(2,128)}, u32[]{:S(2)}) copy-start(f32[384,2]{0,1:T(2,128)} %param.13) | copy-start | bytes 9220
  270.2 35.0 %all-to-all-start.1 = ((bf16[8,192,256]{2,1,0:T(8,128)(2,1)}), bf16[8,192,256]{2,1,0:T(8,128)(2,1)}, u32[]{:S(2)}, u32[]{:S(2)}) async-start(bf16[8,192,256]{2,1,0:T(8,128)(2,1)} %bitcast.46), calls=%async_computation.2 | async-start | bytes 1572864 | tf_op jit(solution)/shard_map/all_to_all | solution.py:201
  299.6 5.6 %copy-start.14 = (s32[384]{0:T(512)S(1)}, s32[384]{0:T(512)}, u32[]{:S(2)}) copy-start(s32[384]{0:T(512)} %copy-done.13) | copy-start | bytes 4612
  299.6 7.5 %copy-start.12 = (s32[384]{0:T(512)S(1)}, s32[384]{0:T(512)}, u32[]{:S(2)}) copy-start(s32[384]{0:T(512)} %copy-done.11) | copy-start | bytes 4612
Sparse Core Ops, SparseCore 0:
  29.4 48.3 all-gather.1
  207.6 62.5 reduce-scatter.1

commit v2 on v1

v2 whole, which is shorter than its diff:
```python
import functools

import jax
import jax.numpy as jnp
from jax import lax
from jax.experimental import pallas as pl
from jax.experimental.pallas import tpu as pltpu
from jax.sharding import PartitionSpec as P

EXPERTS = 8
epsilon = 1e-06
MESH = pl.DeviceIdType.MESH
NZ, NY = 8, 4
VMEM_LIMIT = 54 * 1024 * 1024
PARTS = ((0, 384), (384, 320))


NX = 4
COLS = (((1,), (0,)), ((), ()))
ROWS = (((1,), (1,)), ((), ()))


def whole_kernel(
    g_ref, u_ref, d_ref, gain_ref, tok_ref, row_ref, col_ref, logit_ref,
    og, ou, od, mix_ref,
    scaled, y0, y1, away, xs, xall, inv_ref, hidden, theirs, got, mine, joint, parts, ret, back,
    ysend, yrecv, zsend, zrecv, tsend, trecv, asend, arecv, psend, precv, rsend, rrecv, bsend, brecv,
):
    fs = lax.axis_index("fs")
    tp = lax.axis_index("tp")
    z, y = fs // NY, lax.rem(fs, NY)
    x, core = tp // 2, lax.rem(tp, 2)
    parity = lax.rem(z, 2)
    sources, outs, ybufs = (scaled.at[0], scaled.at[1], d_ref), (og, ou, od), (y0, y1)
    rows = g_ref.shape[2]
    most = xs.shape[1]
    slots = xall.shape[1]
    half_slots = slots // 2
    here = parity * NY + y

    def zat(step):
        return lax.rem(z + step + NZ, NZ)

    def yat(step):
        return lax.rem(y + step + NY, NY)

    def device(dz, dy):
        return {"fs": zat(dz) * NY + yat(dy)}

    def member(flip, dy):
        p = (1 - parity) if flip else parity
        return (z - parity + p) * NY + yat(dy), p * NY + yat(dy)

    def mate(step):
        return {"tp": lax.rem(x + step + NX, NX) * 2 + core}

    partner = {"tp": x * 2 + 1 - core}

    group = [(0, 1), (0, 3), (0, 2), (1, 0), (1, 1), (1, 3), (1, 2)]
    barrier = pltpu.get_barrier_semaphore()
    greeted = [device(0, 1), device(0, 2), device(0, 3)]
    greeted += [device(1, 0), device(-1, 0), device(2, 0), device(-2, 0)]
    greeted += [{"fs": member(1, dy)[0]} for dy in (1, 2, 3)]
    greeted += [{"tp": lax.rem(tp + step, 2 * NX)} for step in range(1, 2 * NX)]
    for other in greeted:
        pl.semaphore_signal(barrier, inc=1, device_id=other, device_id_type=MESH)
    pl.semaphore_wait(barrier, len(greeted))

    units = [(m, h) for m in range(3) for h in range(2)]

    def ycopy(u, dy, to_row):
        m, h = units[u]
        lo, n = PARTS[h]
        return pltpu.make_async_remote_copy(
            src_ref=sources[m].at[:, yat(dy), :, pl.ds(lo, n)],
            dst_ref=ybufs[h].at[m, :, pl.ds(to_row * rows, rows), :],
            send_sem=ysend.at[u * 3 + dy - 1],
            recv_sem=yrecv.at[u * 3 + dy - 1],
            device_id=device(0, dy),
            device_id_type=MESH,
        )

    def zcopy(u, kind, sign, arriving=False):
        m, h = units[u]
        lo, n = PARTS[h]
        out = outs[m]
        near = {"a": 1, "b": 2, "c": 2, "d": 2}[kind]
        hops = {"a": 0, "b": 0, "c": 1, "d": 2}[kind]
        block = zat(-sign * hops)
        if arriving:
            block = zat(-sign * (hops + near))
        if kind == "d":
            half = n // 2
            lo, n = (lo, half) if sign > 0 else (lo + half, half)
        place = out.at[block, pl.ds(lo, n), :]
        source = away.at[m, pl.ds(lo, n), :] if kind == "a" else place
        at = u * 8 + "abcd".index(kind) * 2 + (0 if sign > 0 else 1)
        return pltpu.make_async_remote_copy(
            src_ref=source,
            dst_ref=place,
            send_sem=zsend.at[at],
            recv_sem=zrecv.at[at],
            device_id=device(sign * near, 0),
            device_id_type=MESH,
        )

    def tokens_copy(flip, dy, arriving=False):
        to, expert = member(flip, dy)
        owner = member(flip, -dy)[1] if arriving else here
        at = flip * NY + dy
        return pltpu.make_async_remote_copy(
            src_ref=xs.at[expert],
            dst_ref=xall.at[tp, pl.ds(pl.multiple_of(owner * most, 16), most), :],
            send_sem=tsend.at[at],
            recv_sem=trecv.at[at],
            device_id={"fs": to},
            device_id_type=MESH,
        )

    def gather_copy(step, arriving=False):
        block = lax.rem(x - step + NX, NX) * 2 + core if arriving else tp
        return pltpu.make_async_remote_copy(
            src_ref=xall.at[tp],
            dst_ref=xall.at[block],
            send_sem=asend.at[step],
            recv_sem=arecv.at[step],
            device_id=mate(step),
            device_id_type=MESH,
        )

    def relay_copy(step, arriving=False):
        block = lax.rem(x - step + NX, NX) * 2 + core
        if arriving:
            block = lax.rem(x - step + NX, NX) * 2 + 1 - core
        return pltpu.make_async_remote_copy(
            src_ref=xall.at[block],
            dst_ref=xall.at[block],
            send_sem=asend.at[NX + step],
            recv_sem=arecv.at[NX + step],
            device_id=partner,
            device_id_type=MESH,
        )

    def block_at(k):
        return lax.rem(z + (2 * lax.rem(k, 2) - 1) * ((k + 1) // 2) + NZ, NZ)

    def pair_copy(k):
        return pltpu.make_async_remote_copy(
            src_ref=theirs.at[k],
            dst_ref=got.at[k],
            send_sem=psend.at[k],
            recv_sem=precv.at[k],
            device_id=partner,
            device_id_type=MESH,
        )

    def half_rows(which):
        return pl.ds(pl.multiple_of(which * half_slots, 16), half_slots)

    def sum_copy(k, to, sender):
        return pltpu.make_async_remote_copy(
            src_ref=joint.at[k],
            dst_ref=parts.at[sender // 2, half_rows(lax.rem(sender, 2)), :],
            send_sem=rsend.at[k],
            recv_sem=rrecv.at[sender],
            device_id={"tp": to},
            device_id_type=MESH,
        )

    def back_copy(flip, dy, arriving=False):
        to, owner = member(flip, dy)
        expert = member(flip, -dy)[1] if arriving else here
        at = flip * NY + dy
        return pltpu.make_async_remote_copy(
            src_ref=ret.at[owner],
            dst_ref=back.at[expert],
            send_sem=bsend.at[at],
            recv_sem=brecv.at[at],
            device_id={"fs": to},
            device_id_type=MESH,
        )

    def scale(m, ref):
        gain = gain_ref[...]

        def one(e, carry):
            block = ref[e // NY, lax.rem(e, NY)]
            scaled[m, e // NY, lax.rem(e, NY)] = (block.astype(jnp.float32) * gain).astype(
                jnp.bfloat16
            )
            return carry

        lax.fori_loop(0, EXPERTS, one, 0)

    def across(m):
        for u in (2 * m, 2 * m + 1):
            for dy in (1, 3, 2):
                ycopy(u, dy, y).start()
        for h, (lo, n) in enumerate(PARTS):
            ybufs[h][m, :, pl.ds(y * rows, rows), :] = sources[m][:, y, :, lo : lo + n]

    scale(0, g_ref)
    across(0)

    def pick(e, carry):
        ids = lax.broadcasted_iota(jnp.int32, (most, tok_ref.shape[0]), 0) + e * most
        hit = (ids == row_ref[0:1, :]) | (ids == row_ref[1:2, :])
        chosen = jnp.where(hit, 1.0, 0.0).astype(jnp.bfloat16)
        xs[e] = jnp.dot(chosen, tok_ref[...], preferred_element_type=jnp.float32).astype(
            jnp.bfloat16
        )
        return carry

    lax.fori_loop(0, EXPERTS, pick, 0)
    for flip, dy in group:
        tokens_copy(flip, dy).start()
    xall[tp, pl.ds(pl.multiple_of(here * most, 16), most), :] = xs[here]
    scale(1, u_ref)
    across(1)
    across(2)

    def turn(u):
        m, h = units[u]
        lo, n = PARTS[h]
        for dy in (1, 3, 2):
            ycopy(u, dy, yat(-dy)).wait_recv()
        away[m, pl.ds(lo, n), :] = ybufs[h][m, 1 - parity].T
        outs[m][z, pl.ds(lo, n), :] = ybufs[h][m, parity].T

    def first(u):
        turn(u)
        for kind in "ab":
            for sign in (1, -1):
                zcopy(u, kind, sign).start()

    def second(u):
        for kind, after in (("a", "c"), ("b", "d")):
            for sign in (1, -1):
                zcopy(u, kind, sign, True).wait_recv()
                zcopy(u, after, sign).start()

    def landed(u):
        for kind in "cd":
            for sign in (1, -1):
                zcopy(u, kind, sign, True).wait_recv()

    first(0)
    first(1)
    for flip, dy in group:
        tokens_copy(flip, dy, True).wait_recv()
    for step in (1, 3, 2):
        gather_copy(step).start()
    relay_copy(0).start()
    second(0)
    first(2)
    second(1)
    first(3)
    for step in (1, 3):
        gather_copy(step, True).wait_recv()
        relay_copy(step).start()
    second(2)
    first(4)
    gather_copy(2, True).wait_recv()
    relay_copy(2).start()
    second(3)
    first(5)
    second(4)
    for step in range(NX):
        relay_copy(step, True).wait_recv()

    def norms(i, carry):
        at = pl.ds(pl.multiple_of(i * most, 16), most)
        total = jnp.zeros((most, 1), jnp.float32)
        for block in range(xall.shape[0]):
            v = xall[block, at, :].astype(jnp.float32)
            total = total + jnp.sum(v * v, axis=1, keepdims=True)
        mean = total / (xall.shape[0] * xall.shape[2])
        inv_ref[at, :] = lax.rsqrt(mean + epsilon)
        return carry

    lax.fori_loop(0, EXPERTS, norms, 0)
    for u in range(4):
        landed(u)

    tile = slots // 4

    def hide(i, carry):
        at = pl.ds(pl.multiple_of(i * tile, 16), tile)
        gate = jnp.zeros((tile, og.shape[1]), jnp.float32)
        up = jnp.zeros((tile, og.shape[1]), jnp.float32)
        for block in range(NZ):
            v = xall[block, at, :]
            gate = gate + lax.dot_general(v, og[block], ROWS, preferred_element_type=jnp.float32)
            up = up + lax.dot_general(v, ou[block], ROWS, preferred_element_type=jnp.float32)
        inverse = inv_ref[at, :]
        gate = gate * inverse
        up = up * inverse
        hidden[at, :] = (gate / (1.0 + jnp.exp(-gate)) * up).astype(jnp.bfloat16)
        return carry

    lax.fori_loop(0, slots // tile, hide, 0)
    second(5)

    def project(k, carry):
        weights = od[block_at(k)]
        theirs[k] = lax.dot_general(
            hidden[half_rows(1 - core), :], weights, COLS, preferred_element_type=jnp.float32
        ).astype(jnp.bfloat16)
        pair_copy(k).start()
        mine[k] = lax.dot_general(
            hidden[half_rows(core), :], weights, COLS, preferred_element_type=jnp.float32
        ).astype(jnp.bfloat16)
        return carry

    def join(k, carry):
        to = block_at(k)
        pair_copy(k).wait_recv()
        joint[k] = (mine[k].astype(jnp.float32) + got[k].astype(jnp.float32)).astype(jnp.bfloat16)

        @pl.when(to != tp)
        def _():
            sum_copy(k, to, tp).start()

        @pl.when(to == tp)
        def _():
            parts[x, half_rows(core), :] = joint[k]

        return carry

    lax.fori_loop(0, 5, project, 0)
    lax.fori_loop(0, 5, join, 0)
    landed(4)
    landed(5)
    lax.fori_loop(5, NZ, project, 0)
    lax.fori_loop(5, NZ, join, 0)

    for step in range(1, 2 * NX):
        sender = lax.rem(tp + step, 2 * NX)
        sum_copy(0, sender, sender).wait_recv()

    def total(owner):
        at = pl.ds(pl.multiple_of(owner * most, 16), most)
        value = parts[0, at, :].astype(jnp.float32)
        for block in range(1, NX):
            value = value + parts[block, at, :].astype(jnp.float32)
        ret[owner] = value.astype(jnp.bfloat16)

    for flip, dy in group:
        total(member(flip, dy)[1])
        back_copy(flip, dy).start()
    total(here)
    back[here] = ret[here]
    for flip, dy in group:
        back_copy(flip, dy, True).wait_recv()

    count = tok_ref.shape[0]
    piece = count // 3

    def mix(i, carry):
        at = pl.ds(pl.multiple_of(i * piece, 16), piece)
        ids = lax.broadcasted_iota(jnp.int32, (piece, slots), 1)
        results = back[...].reshape(slots, back.shape[2])
        wanted = col_ref[at, :]
        scores = logit_ref[at, :]
        value = jnp.zeros((piece, back.shape[2]), jnp.float32)
        for k in range(2):
            chosen = jnp.where(ids == wanted[:, k : k + 1], 1.0, 0.0).astype(jnp.bfloat16)
            picked = jnp.dot(chosen, results, preferred_element_type=jnp.float32)
            value = value + picked * jax.nn.sigmoid(
                scores[:, k : k + 1] - scores[:, 1 - k : 2 - k]
            )
        mix_ref[at, :] = value.astype(jnp.bfloat16)
        return carry

    lax.fori_loop(0, count // piece, mix, 0)

    for u in range(6):
        for dy in (1, 3, 2):
            ycopy(u, dy, y).wait_send()
        for kind in "abcd":
            for sign in (1, -1):
                zcopy(u, kind, sign).wait_send()
    for flip, dy in group:
        tokens_copy(flip, dy).wait_send()
        back_copy(flip, dy).wait_send()
    for step in range(1, NX):
        gather_copy(step).wait_send()
    for step in range(NX):
        relay_copy(step).wait_send()

    def sent(k, carry):
        pair_copy(k).wait_send()
        to = block_at(k)

        @pl.when(to != tp)
        def _():
            sum_copy(k, to, tp).wait_send()

        return carry

    lax.fori_loop(0, NZ, sent, 0)


def whole(gate, up, down, gain, tokens, slots, logits):
    _, rows, width = gate.shape
    count, features = tokens.shape
    most = count // 2
    split = [w.reshape(2, NY, rows, width) for w in (gate, up, down)]
    out = jax.ShapeDtypeStruct((NZ, width, NY * rows), jnp.bfloat16)
    dma = pltpu.SemaphoreType.DMA
    vmem = lambda *shape, dtype=jnp.bfloat16: pltpu.VMEM(shape, dtype)
    total = EXPERTS * most
    return pl.pallas_call(
        whole_kernel,
        out_shape=(out, out, out, jax.ShapeDtypeStruct((count, features), jnp.bfloat16)),
        in_specs=[pl.BlockSpec(memory_space=pltpu.VMEM)] * 8,
        out_specs=(pl.BlockSpec(memory_space=pltpu.VMEM),) * 4,
        scratch_shapes=[
            vmem(2, 2, NY, rows, width),
            vmem(3, 2, NY * rows, PARTS[0][1]),
            vmem(3, 2, NY * rows, PARTS[1][1]),
            vmem(3, width, NY * rows),
            vmem(EXPERTS, most, features),
            vmem(2 * NX, total, features),
            vmem(total, 1, dtype=jnp.float32),
            vmem(total, width),
            vmem(NZ, total // 2, features),
            vmem(NZ, total // 2, features),
            vmem(NZ, total // 2, features),
            vmem(NZ, total // 2, features),
            vmem(NX, total, features),
            vmem(EXPERTS, most, features),
            vmem(EXPERTS, most, features),
            dma((18,)), dma((18,)), dma((48,)), dma((48,)), dma((8,)), dma((8,)), dma((8,)), dma((8,)),
            dma((8,)), dma((8,)), dma((8,)), dma((8,)), dma((8,)), dma((8,)),
        ],
        compiler_params=pltpu.CompilerParams(
            collective_id=0, has_side_effects=True, vmem_limit_bytes=VMEM_LIMIT
        ),
        cost_estimate=pl.CostEstimate(flops=10**11, bytes_accessed=10**7, transcendentals=0),
    )(*split, gain, tokens, slots, slots.T, logits)


def place_kernel(g_ref, u_ref, d_ref, og, ou, od, sem):
    copies = []
    for m, (ref, out) in enumerate(((g_ref, og), (u_ref, ou), (d_ref, od))):
        for block in range(NZ):
            size = ref.shape[2]
            copies.append(
                pltpu.make_async_copy(
                    ref.at[block], out.at[:, pl.ds(block * size, size)], sem.at[m * NZ + block]
                )
            )
    for copy in copies:
        copy.start()
    for copy in copies:
        copy.wait()


def placed_out(blocks):
    nz, width, size = blocks[0].shape
    out = jax.ShapeDtypeStruct((width, nz * size), jnp.bfloat16)
    done = pl.pallas_call(
        place_kernel,
        out_shape=(out,) * 3,
        in_specs=[pl.BlockSpec(memory_space=pltpu.VMEM)] * 3,
        out_specs=(pl.BlockSpec(memory_space=pl.ANY),) * 3,
        scratch_shapes=[pltpu.SemaphoreType.DMA((3 * NZ,))],
    )(*blocks)
    return [o.T[None] for o in done]


def slot_plan(routes, most):
    experts_all = jnp.arange(EXPERTS, dtype=jnp.int32)
    named = (routes.T[:, None, :] == experts_all[None, :, None]).astype(jnp.bfloat16)
    tokens = routes.shape[0]
    places = jnp.arange(tokens)
    before = (places[:, None] < places[None, :]).astype(jnp.bfloat16)
    rank = jnp.dot(named.reshape(-1, tokens), before, preferred_element_type=jnp.float32)
    rank = rank.reshape(named.shape)
    count = jnp.sum(named[0].astype(jnp.float32), axis=1)
    rank = rank + jnp.stack([jnp.zeros_like(count), count])[:, :, None]
    slot = rank + most * experts_all[None, :, None].astype(jnp.float32)
    return jnp.sum(jnp.where(named > 0, slot, 0.0), axis=1).astype(jnp.int32)


def shards(tokens, norm_gain, gate_train, up_train, down_train, routes, route_logits):
    slots = slot_plan(routes, tokens.shape[0] // 2)
    *blocks, mixed = whole(
        gate_train, up_train, down_train, norm_gain[:, None], tokens, slots, route_logits
    )
    return (*placed_out(blocks), mixed)


def solution(mesh):
    placed = (
        P("fs", "tp"),
        P("fs"),
        P(None, "fs", "tp"),
        P(None, "fs", "tp"),
        P(None, "fs", "tp"),
        P("fs", None),
        P("fs", None),
    )
    return jax.shard_map(
        shards,
        mesh=mesh,
        in_specs=placed,
        out_specs=(P("fs", None, "tp"), P("fs", None, "tp"), P("fs", None, "tp"), P("fs", "tp")),
        check_vma=False,
    )
```

time: 319 us -> 231 us (0.72)
  Pallas kernels: 135 us -> 224 us
  waiting for transfers between devices: 72.6 us -> 0 us
  local copies, waits for them, and re-layouts: 42.6 us -> 4.39 us
  matrix products: 34.5 us -> 0.93 us
  between operations: 14.2 us -> 0.69 us
  starting transfers between devices: 10.6 us -> 0 us
  other arithmetic: 6.85 us -> 0.82 us
    pallas_call x1 -> x2, Pallas kernels: 135 us -> 224 us  [the longest x1 217 us: whole(): pl.pallas_call(whole_kernel, out_shape=(out, out, out, jax.ShapeDtypeStru...]
    reduce_scatter x1 -> x0, waiting for transfers between devices: 62.7 us -> none  [shards(): lax.psum_scatter(lax.dot_general(active, down_out[0], (((1,), (1,)), ((),...]
    dot_general x5 -> x0, matrix products: 33.6 us -> none  [the longest x1 19.1 us: shards(): lax.dot_general(active, down_out[0], (((1,), (1,)), ((), ())), preferred_...]
    reshape x3 -> x0, local copies, waits for them, and re-layouts: 16.7 us -> none  [shards(): w.transpose(0, 2, 1).reshape(1, -1, gate_train.shape[2])]
    transpose x3 -> x0, local copies, waits for them, and re-layouts: 13.2 us -> none  [shards(): w.transpose(0, 2, 1).reshape(1, -1, gate_train.shape[2])]
    all_to_all x2 -> x0, starting transfers between devices: 10.5 us -> none  [the longest x1 5.55 us: shards(): lax.all_to_all(outgoing, 'fs', split_axis=0, concat_axis=0, tiled=True, a...]
    all_to_all x2 -> x0, waiting for transfers between devices: 9.84 us -> none  [the longest x1 9.84 us: shards(): lax.all_to_all(outgoing, 'fs', split_axis=0, concat_axis=0, tiled=True, a...]
    another operation x3 -> x0, local copies, waits for them, and re-layouts: 6.19 us -> none  [the longest x1 2.21 us: shards(): gate_val = jnp.dot(normed, gate_out[0], preferred_element_type=jnp.float32)]
  transfers between devices with their start and end apart: 4 -> 0, of which waited for: 2 -> 0; matrix products, arithmetic and copies ran while one was open for 12% -> 0% of each run, Pallas kernels for 43% -> 0%
where the time goes in v2:
time: 231 us
  Pallas kernels  224 us (97%)
  local copies, waits for them, and re-layouts  4.39 us (2%)
    pallas_call x1, Pallas kernels, whole(): pl.pallas_call(whole_kernel, out_shape=(out, out, out, jax.ShapeDtypeStru...  217 us
    pallas_call x1, Pallas kernels, placed_out(): pl.pallas_call(place_kernel, out_shape=(out,) * 3, in_specs=[pl.BlockSpec...  7.12 us

profile of v2, /device:TPU:5, one launch (start us, length us, event | category | flops | bytes accessed | tf_op | source)
XLA Modules:
  0.0 230.6 jit_solution(13657716057133299357)
XLA Ops:
  0.6 0.7 fusion.5
  1.3 0.1 convert_reduce_fusion
  1.5 0.9 fusion.2
  2.4 0.0 copy-start.1
  2.4 1.4 copy.19.gain_ref
  3.8 0.8 copy.18
  4.6 1.5 copy.20.logit_ref
  6.1 0.0 copy-done.1
  6.1 216.7 %shard_map.102 = (bf16[8,704,256]{2,1,0:T(8,128)(2,1)}, bf16[8,704,256]{2,1,0:T(8,128)(2,1)}, bf16[8,704,256]{2,1,0:T(8,128)(2,1)}, bf16[384,256]{1,0:T(8,128)(2,1)}) custom-call(bf16[2,4,64,704]{3,2,1,0:T(8,128)(2,1)} %bitcast.27, bf16[2,4,64,704]{3,2,1,0:T(8,128)(2,1)} %bitcast.28, bf16[2,4,64,704]{3,2,1,0:T(8,128)(2,1)} %bitcast.29, ...), custom_call_target="tpu_custom_call" | custom-call | flops 99999997952 | bytes 10000000 | tf_op jit(solution)/shard_map/pallas_call | solution.py:413
  222.8 0.0 copy-start
  222.8 7.1 %shard_map.103 = (bf16[704,2048]{1,0:T(8,128)(2,1)}, bf16[704,2048]{1,0:T(8,128)(2,1)}, bf16[704,2048]{1,0:T(8,128)(2,1)}) custom-call(bf16[8,704,256]{2,1,0:T(8,128)(2,1)} %get-tuple-element.11.g_ref, bf16[8,704,256]{2,1,0:T(8,128)(2,1)} %get-tuple-element.12.u_ref, bf16[8,704,256]{2,1,0:T(8,128)(2,1)} %get-tuple-element.13.d_ref), custom_call_target="tpu_custom_call" | custom-call | tf_op jit(solution)/shard_map/pallas_call | solution.py:463
  229.9 0.0 copy-done
  230.0 0.7 copy.22
  (3 shorter events, 0.0 us)
Async XLA Ops:
  2.4 3.7 %copy-start.1 = (s32[2,384]{1,0:T(2,128)}, s32[2,384]{1,0:T(2,128)S(1)}, u32[]{:S(2)}) copy-start(s32[2,384]{1,0:T(2,128)S(1)} %convert_element_type.24.row_ref) | copy-start | bytes 9220
  222.8 7.1 %copy-start = (bf16[384,256]{1,0:T(8,128)(2,1)S(1)}, bf16[384,256]{1,0:T(8,128)(2,1)}, u32[]{:S(2)}) copy-start(bf16[384,256]{1,0:T(8,128)(2,1)} %get-tuple-element.25) | copy-start | bytes 589828

commit v3 on v2

v3 whole, which is shorter than its diff:
```python
import functools

import jax
import jax.numpy as jnp
from jax import lax
from jax.experimental import pallas as pl
from jax.experimental.pallas import tpu as pltpu
from jax.sharding import PartitionSpec as P

EXPERTS = 8
epsilon = 1e-06
MESH = pl.DeviceIdType.MESH
NZ, NY = 8, 4
VMEM_LIMIT = 60 * 1024 * 1024
NZ, NY, NX = 8, 4, 4
LANES = 128
SPLIT = ((0, 0, 128), (0, 128, 256), (0, 384, 320), (1, 0, 384), (1, 384, 320))
DOWN = ((2, 0, 384), (2, 384, 320))
ACROSS = SPLIT + DOWN
UNITS = len(SPLIT) + 2
COLS = (((1,), (0,)), ((), ()))
ROWS = (((1,), (1,)), ((), ()))
FULL = 5


def whole_kernel(
    g_in, u_in, d_in, gain_in, tok_in, route_in, logit_in,
    g_out, u_out, d_out, mix_ref,
    og, ou, od, g_ref, u_ref, d_ref, gain_ref, tok_ref, route_ref, logit_ref, scaled, ybuf, away, awayd, slot_ref, xs, xall, inv_ref, hidden,
    theirs, got, mine, joint, far, theirs_h, got_h, mine_h, joint_h, far_h, parts, ret, back,
    ysend, yrecv, zsend, zrecv, tsend, trecv, asend, arecv, psend, precv, fsend, frecv, rrecv, bsend, brecv, lsem, osem,
):
    fs = lax.axis_index("fs")
    tp = lax.axis_index("tp")
    z, y = fs // NY, lax.rem(fs, NY)
    x, core = tp // 2, lax.rem(tp, 2)
    parity = lax.rem(z, 2)
    sources = (scaled.at[0], scaled.at[1], d_ref)
    rows = g_ref.shape[2]
    width = g_ref.shape[3]
    most = xs.shape[1]
    few = most // 2
    slots = xall.shape[1]
    half_slots = slots // 2
    quarter = slots // 4
    here = parity * NY + y

    def zat(step):
        return lax.rem(z + step + NZ, NZ)

    def yat(step):
        return lax.rem(y + step + NY, NY)

    def device(dz, dy):
        return {"fs": zat(dz) * NY + yat(dy)}

    def mate(step):
        return {"tp": lax.rem(x + step + NX, NX) * 2 + core}

    partner = {"tp": x * 2 + 1 - core}
    group = [(dz, dy) for dz, dys in ((1, (0, 1, 3, 2)), (-1, (0, 1, 3, 2)), (0, (1, 3, 2))) for dy in dys]

    loads = [
        pltpu.make_async_copy(source, held, lsem.at[i])
        for i, (source, held) in enumerate(
            (
                (g_in, g_ref),
                (gain_in, gain_ref),
                (route_in, route_ref),
                (tok_in, tok_ref),
                (u_in, u_ref),
                (d_in, d_ref),
                (logit_in, logit_ref),
            )
        )
    ]
    for load in loads:
        load.start()
    barrier = pltpu.get_barrier_semaphore()
    greeted = [device(dz, dy) for dz, dy in group + [(2, 0), (-2, 0)]]
    greeted += [{"tp": lax.rem(tp + step, 2 * NX)} for step in range(1, 2 * NX)]
    for other in greeted:
        pl.semaphore_signal(barrier, inc=1, device_id=other, device_id_type=MESH)
    pl.semaphore_wait(barrier, len(greeted))

    def ycopy(u, dy, to_row):
        m, lo, n = ACROSS[u]
        return pltpu.make_async_remote_copy(
            src_ref=sources[m].at[:, yat(dy), :, pl.ds(lo, n)],
            dst_ref=ybuf.at[m, :, pl.ds(to_row * rows, rows), pl.ds(lo, n)],
            send_sem=ysend.at[u * 3 + dy - 1],
            recv_sem=yrecv.at[u * 3 + dy - 1],
            device_id=device(0, dy),
            device_id_type=MESH,
        )

    def zcopy(u, kind, sign, arriving=False):
        if u < len(SPLIT):
            m, lo, n = SPLIT[u]
            out, left = (og, ou)[m], away.at[m]
        else:
            lo, n = 0, width
            out, left = od.at[u - len(SPLIT)], awayd.at[u - len(SPLIT)]
        near = {"a": 1, "b": 2, "c": 2, "d": 2}[kind]
        hops = {"a": 0, "b": 0, "c": 1, "d": 2}[kind]
        block = zat(-sign * hops)
        if arriving:
            block = zat(-sign * (hops + near))
        if kind == "d":
            half = n // 2
            lo, n = (lo, half) if sign > 0 else (lo + half, half)
        place = out.at[block, pl.ds(lo, n), :]
        source = left.at[pl.ds(lo, n), :] if kind == "a" else place
        at = u * 8 + "abcd".index(kind) * 2 + (0 if sign > 0 else 1)
        return pltpu.make_async_remote_copy(
            src_ref=source,
            dst_ref=place,
            send_sem=zsend.at[at],
            recv_sem=zrecv.at[at],
            device_id=device(sign * near, 0),
            device_id_type=MESH,
        )

    def base(dz):
        return {0: 0, 1: half_slots, -1: half_slots + quarter}[dz]

    def arrived_rows(dz, at_y):
        n = few if dz else most
        return pl.ds(pl.multiple_of(base(dz) + at_y * n, 16), n)

    def held_rows(dz):
        return pl.ds({0: 0, 1: 0, -1: few}[dz], few if dz else most)

    def expert(dz, at_y):
        return ((1 - parity) if dz else parity) * NY + at_y

    def tokens_copy(dz, dy, arriving=False):
        at = (dz + 1) * NY + dy
        return pltpu.make_async_remote_copy(
            src_ref=xs.at[expert(dz, yat(dy)), held_rows(dz), :],
            dst_ref=xall.at[tp, arrived_rows(dz, yat(-dy) if arriving else y), :],
            send_sem=tsend.at[at],
            recv_sem=trecv.at[at],
            device_id=device(dz, dy),
            device_id_type=MESH,
        )

    def back_copy(dz, dy, arriving=False):
        at = (dz + 1) * NY + dy
        owner = expert(dz, yat(-dy)) if arriving else here
        return pltpu.make_async_remote_copy(
            src_ref=ret.at[arrived_rows(dz, yat(dy)), :],
            dst_ref=back.at[owner, held_rows(dz), :],
            send_sem=bsend.at[at],
            recv_sem=brecv.at[at],
            device_id=device(-dz, dy),
            device_id_type=MESH,
        )

    def gather_copy(step, arriving=False):
        block = lax.rem(x - step + NX, NX) * 2 + core if arriving else tp
        return pltpu.make_async_remote_copy(
            src_ref=xall.at[tp],
            dst_ref=xall.at[block],
            send_sem=asend.at[step],
            recv_sem=arecv.at[step],
            device_id=mate(step),
            device_id_type=MESH,
        )

    def relay_copy(step, arriving=False):
        block = lax.rem(x - step + NX, NX) * 2 + core
        if arriving:
            block = lax.rem(x - step + NX, NX) * 2 + 1 - core
        return pltpu.make_async_remote_copy(
            src_ref=xall.at[block],
            dst_ref=xall.at[block],
            send_sem=asend.at[NX + step],
            recv_sem=arecv.at[NX + step],
            device_id=partner,
            device_id_type=MESH,
        )

    def scale(m, ref):
        wide = gain_ref[...]
        on = lax.broadcasted_iota(jnp.int32, (rows, rows), 0) == lax.broadcasted_iota(
            jnp.int32, (rows, rows), 1
        )
        gain = jnp.sum(jnp.where(on, wide, 0.0), axis=1, keepdims=True)

        def one(e, carry):
            block = ref[e // NY, lax.rem(e, NY)]
            scaled[m, e // NY, lax.rem(e, NY)] = (block.astype(jnp.float32) * gain).astype(
                jnp.bfloat16
            )
            return carry

        lax.fori_loop(0, EXPERTS, one, 0)

    def across(m):
        for u, (owner, lo, n) in enumerate(ACROSS):
            if owner == m:
                for dy in (1, 3, 2):
                    ycopy(u, dy, y).start()
        ybuf[m, :, pl.ds(y * rows, rows), :] = sources[m][:, y]

    def plan():
        count = tok_ref.shape[0]
        lines = lax.broadcasted_iota(jnp.int32, (2 * EXPERTS, count), 0)
        routes = route_ref[...]
        named = (routes[0:1, :] == lines) | (routes[1:2, :] == lines - EXPERTS)
        named = jnp.where(named, 1.0, 0.0)
        before = jnp.where(
            lax.broadcasted_iota(jnp.int32, (count, count), 0)
            < lax.broadcasted_iota(jnp.int32, (count, count), 1),
            1.0,
            0.0,
        )
        rank = jnp.dot(
            named.astype(jnp.bfloat16),
            before.astype(jnp.bfloat16),
            preferred_element_type=jnp.float32,
        )
        for k in range(2):
            one = named[k * EXPERTS : (k + 1) * EXPERTS]
            place = rank[k * EXPERTS : (k + 1) * EXPERTS]
            if k:
                place = place + jnp.sum(named[:EXPERTS], axis=1, keepdims=True)
            place = place + (lines[:EXPERTS] * most).astype(jnp.float32)
            slot = jnp.sum(one * place, axis=0, keepdims=True)
            slot_ref[k : k + 1, :] = slot.astype(jnp.int32)

    for load in loads[:2]:
        load.wait()
    scale(0, g_ref)
    across(0)
    for load in loads[2:]:
        load.wait()
    plan()

    def pick(e, carry):
        ids = lax.broadcasted_iota(jnp.int32, (most, tok_ref.shape[0]), 0) + e * most
        hit = (ids == slot_ref[0:1, :]) | (ids == slot_ref[1:2, :])
        chosen = jnp.where(hit, 1.0, 0.0).astype(jnp.bfloat16)
        xs[e] = jnp.dot(chosen, tok_ref[...], preferred_element_type=jnp.float32).astype(
            jnp.bfloat16
        )
        return carry

    lax.fori_loop(0, EXPERTS, pick, 0)
    for dz, dy in group:
        tokens_copy(dz, dy).start()
    xall[tp, arrived_rows(0, y), :] = xs[here]
    scale(1, u_ref)
    across(1)
    across(2)

    def turn(u):
        if u < len(SPLIT):
            m, lo, n = SPLIT[u]
            for dy in (1, 3, 2):
                ycopy(u, dy, yat(-dy)).wait_recv()
            away[m, pl.ds(lo, n), :] = ybuf[m, 1 - parity, :, lo : lo + n].T
            (og, ou)[m][z, pl.ds(lo, n), :] = ybuf[m, parity, :, lo : lo + n].T
        elif u == len(SPLIT):
            for part, (m, lo, n) in enumerate(DOWN):
                for dy in (1, 3, 2):
                    ycopy(u + part, dy, yat(-dy)).wait_recv()
                gone = ybuf[m, 1 - parity, :, lo : lo + n].T
                kept = ybuf[m, parity, :, lo : lo + n].T
                for f in range(2):
                    awayd[f, pl.ds(lo, n), :] = gone[:, f * LANES : (f + 1) * LANES]
                    od[f, z, pl.ds(lo, n), :] = kept[:, f * LANES : (f + 1) * LANES]

    def first(u):
        turn(u)
        for kind in "ab":
            for sign in (1, -1):
                zcopy(u, kind, sign).start()

    def second(u):
        for kind, after in (("a", "c"), ("b", "d")):
            for sign in (1, -1):
                zcopy(u, kind, sign, True).wait_recv()
                zcopy(u, after, sign).start()

    def landed(u):
        for kind in "cd":
            for sign in (1, -1):
                zcopy(u, kind, sign, True).wait_recv()

    first(0)
    first(1)
    second(0)
    for dz, dy in group:
        tokens_copy(dz, dy, True).wait_recv()
    for step in (1, 3, 2):
        gather_copy(step).start()
    relay_copy(0).start()
    first(2)
    second(1)
    first(3)
    second(2)
    first(4)
    for step in (1, 3):
        gather_copy(step, True).wait_recv()
        relay_copy(step).start()
    second(3)
    first(5)
    gather_copy(2, True).wait_recv()
    relay_copy(2).start()
    second(4)
    first(6)
    second(5)
    for step in range(NX):
        relay_copy(step, True).wait_recv()

    def norms(i, carry):
        at = pl.ds(pl.multiple_of(i * most, 16), most)
        total = jnp.zeros((most, 1), jnp.float32)
        for block in range(xall.shape[0]):
            v = xall[block, at, :].astype(jnp.float32)
            total = total + jnp.sum(v * v, axis=1, keepdims=True)
        mean = total / (xall.shape[0] * xall.shape[2])
        inv_ref[at, :] = lax.rsqrt(mean + epsilon)
        return carry

    lax.fori_loop(0, EXPERTS, norms, 0)
    for u in range(5):
        landed(u)

    def written(m, f=0):
        copies = []
        for block in range(NZ):
            if m < 2:
                source, at, n = (og, ou)[m].at[block], block * 2 * LANES, 2 * LANES
            else:
                source, at, n = od.at[f, block], (block * 2 + f) * LANES, LANES
            out = (g_out, u_out, d_out)[m].at[:, pl.ds(at, n)]
            copies.append(pltpu.make_async_copy(source, out, osem.at[(m + f) * NZ + block]))
        return copies

    for m in range(2):
        for copy in written(m):
            copy.start()

    tile = slots // 4

    def hide(i, carry):
        at = pl.ds(pl.multiple_of(i * tile, 16), tile)
        gate = jnp.zeros((tile, width), jnp.float32)
        up = jnp.zeros((tile, width), jnp.float32)
        for block in range(NZ):
            v = xall[block, at, :]
            gate = gate + lax.dot_general(v, og[block], ROWS, preferred_element_type=jnp.float32)
            up = up + lax.dot_general(v, ou[block], ROWS, preferred_element_type=jnp.float32)
        inverse = inv_ref[at, :]
        gate = gate * inverse
        up = up * inverse
        hidden[at, :] = (gate / (1.0 + jnp.exp(-gate)) * up).astype(jnp.bfloat16)
        return carry

    lax.fori_loop(0, slots // tile, hide, 0)
    second(6)

    def block_at(k):
        return lax.rem(z + (2 * lax.rem(k, 2) - 1) * ((k + 1) // 2) + NZ, NZ)

    def half_rows(which):
        return pl.ds(pl.multiple_of(which * half_slots, 16), half_slots)

    def quarter_rows(which, q):
        return pl.ds(pl.multiple_of(which * half_slots + q * quarter, 16), quarter)

    full = (theirs, got, mine, joint, far)
    thin = (theirs_h, got_h, mine_h, joint_h, far_h)

    def lanes(f):
        return pl.ds(0, 2 * LANES) if f is None else pl.ds(f * LANES, LANES)

    def spot(k, f):
        if f is None:
            return full, k, k
        at = k - FULL + f * (NZ - FULL)
        return thin, at, at + FULL

    def pair_copy(k, f):
        bufs, at, sem = spot(k, f)
        return pltpu.make_async_remote_copy(
            src_ref=bufs[0].at[at],
            dst_ref=bufs[1].at[at],
            send_sem=psend.at[sem],
            recv_sem=precv.at[sem],
            device_id=partner,
            device_id_type=MESH,
        )

    def home_copy(k, f):
        bufs, at, sem = spot(k, f)
        return pltpu.make_async_remote_copy(
            src_ref=bufs[3].at[at],
            dst_ref=parts.at[0, half_rows(core), lanes(f)],
            send_sem=fsend.at[sem * 2],
            recv_sem=rrecv.at[8],
            device_id=partner,
            device_id_type=MESH,
        )

    def far_copy(k, f, q):
        bufs, at, sem = spot(k, f)
        return pltpu.make_async_remote_copy(
            src_ref=bufs[3].at[at, pl.ds(q * quarter, quarter), :],
            dst_ref=bufs[4].at[at],
            send_sem=fsend.at[sem * 2 + q],
            recv_sem=frecv.at[sem * 2 + q],
            device_id=mate(1 - 2 * q),
            device_id_type=MESH,
        )

    def near_copy(k, f, q, side):
        bufs, at, sem = spot(k, f)
        return pltpu.make_async_remote_copy(
            src_ref=bufs[3].at[at, pl.ds(q * quarter, quarter), :],
            dst_ref=parts.at[1 + side, quarter_rows(core, q), lanes(f)],
            send_sem=fsend.at[sem * 2 + q],
            recv_sem=rrecv.at[side * 4 + core * 2 + q],
            device_id={"tp": block_at(k)},
            device_id_type=MESH,
        )

    def role(k):
        to = block_at(k)
        return to, lax.rem(to // 2 - x + NX, NX)

    def project(k, f):
        bufs, at, _ = spot(k, f)
        block = block_at(k)
        if f is None:
            weights = jnp.concatenate([od[0, block], od[1, block]], axis=1)
        else:
            weights = od[f, block]
        bufs[0][at] = lax.dot_general(
            hidden[half_rows(1 - core), :], weights, COLS, preferred_element_type=jnp.float32
        ).astype(jnp.bfloat16)
        pair_copy(k, f).start()
        bufs[2][at] = lax.dot_general(
            hidden[half_rows(core), :], weights, COLS, preferred_element_type=jnp.float32
        ).astype(jnp.bfloat16)

    def join(k, f):
        bufs, at, _ = spot(k, f)
        to, which = role(k)
        pair_copy(k, f).wait_recv()
        bufs[3][at] = (
            bufs[2][at].astype(jnp.float32) + bufs[1][at].astype(jnp.float32)
        ).astype(jnp.bfloat16)

        @pl.when(to == tp)
        def _():
            parts[0, half_rows(core), lanes(f)] = bufs[3][at]

        @pl.when((which == 0) & (to != tp))
        def _():
            home_copy(k, f).start()

        @pl.when(which == 2)
        def _():
            far_copy(k, f, 0).start()
            far_copy(k, f, 1).start()

        @pl.when(which == 1)
        def _():
            near_copy(k, f, 1, 0).start()

        @pl.when(which == 3)
        def _():
            near_copy(k, f, 0, 1).start()

    def pass_on(k, f):
        bufs, at, _ = spot(k, f)
        _, which = role(k)
        for when, q, side in ((1, 0, 0), (3, 1, 1)):

            @pl.when(which == when)
            def _():
                far_copy(k, f, q).wait_recv()
                piece = pl.ds(q * quarter, quarter)
                bufs[3][at, piece, :] = (
                    bufs[3][at, piece, :].astype(jnp.float32) + bufs[4][at].astype(jnp.float32)
                ).astype(jnp.bfloat16)
                near_copy(k, f, q, side).start()

    def sent(k, f):
        to, which = role(k)
        pair_copy(k, f).wait_send()

        @pl.when((which == 0) & (to != tp))
        def _():
            home_copy(k, f).wait_send()

        @pl.when(which != 0)
        def _():
            far_copy(k, f, 0).wait_send()
            far_copy(k, f, 1).wait_send()

    def over(what, f):
        lo, hi = (0, FULL) if f is None else (FULL, NZ)

        def step(k, carry):
            what(k, f)
            return carry

        lax.fori_loop(lo, hi, step, 0)

    over(project, None)
    over(join, None)
    landed(5)
    over(project, 0)
    over(join, 0)
    over(pass_on, None)
    landed(6)
    over(project, 1)
    for f in range(2):
        for copy in written(2, f):
            copy.start()
    over(join, 1)
    over(pass_on, 0)
    over(pass_on, 1)

    def whole_wait(place, sem):
        pltpu.make_async_remote_copy(
            src_ref=place,
            dst_ref=place,
            send_sem=fsend.at[0],
            recv_sem=rrecv.at[sem],
            device_id=partner,
            device_id_type=MESH,
        ).wait_recv()

    whole_wait(parts.at[0, half_rows(1 - core), :], 8)
    for side in range(2):
        for c in range(2):
            for q in range(2):
                whole_wait(parts.at[1 + side, quarter_rows(c, q), :], side * 4 + c * 2 + q)

    def total(at):
        value = parts[0, at, :].astype(jnp.float32)
        for block in range(1, 3):
            value = value + parts[block, at, :].astype(jnp.float32)
        ret[at, :] = value.astype(jnp.bfloat16)

    for dz, dy in group:
        total(arrived_rows(dz, yat(dy)))
        back_copy(dz, dy).start()
    total(arrived_rows(0, y))
    back[here] = ret[arrived_rows(0, y), :]
    for dz, dy in group:
        back_copy(dz, dy, True).wait_recv()

    count = tok_ref.shape[0]
    piece = count // 3

    def mix(i, carry):
        ids = lax.broadcasted_iota(jnp.int32, (piece, slots), 1)
        on = lax.broadcasted_iota(jnp.int32, (piece, count), 1) == (
            lax.broadcasted_iota(jnp.int32, (piece, count), 0) + i * piece
        )

        def column(line):
            return jnp.sum(jnp.where(on, line, 0.0), axis=1, keepdims=True)

        results = back[...].reshape(slots, back.shape[2])
        scores = [column(logit_ref[k : k + 1, :]) for k in range(2)]
        value = jnp.zeros((piece, back.shape[2]), jnp.float32)
        for k in range(2):
            wanted = column(slot_ref[k : k + 1, :].astype(jnp.float32)).astype(jnp.int32)
            chosen = jnp.where(ids == wanted, 1.0, 0.0).astype(jnp.bfloat16)
            picked = jnp.dot(chosen, results, preferred_element_type=jnp.float32)
            value = value + picked * jax.nn.sigmoid(scores[k] - scores[1 - k])
        mix_ref[pl.ds(pl.multiple_of(i * piece, 16), piece), :] = value.astype(jnp.bfloat16)
        return carry

    lax.fori_loop(0, count // piece, mix, 0)

    for u in range(UNITS):
        for dy in (1, 3, 2):
            ycopy(u, dy, y).wait_send()
        for kind in "abcd":
            for sign in (1, -1):
                zcopy(u, kind, sign).wait_send()
    for dz, dy in group:
        tokens_copy(dz, dy).wait_send()
        back_copy(dz, dy).wait_send()
    for step in range(1, NX):
        gather_copy(step).wait_send()
    for step in range(NX):
        relay_copy(step).wait_send()
    for f in (None, 0, 1):
        over(sent, f)
    for m, f in ((0, 0), (1, 0), (2, 0), (2, 1)):
        for copy in written(m, f):
            copy.wait()


def whole(gate, up, down, gain, tokens, routes, logits):
    _, rows, width = gate.shape
    count, features = tokens.shape
    most = count // 2
    split = [w.reshape(2, NY, rows, width) for w in (gate, up, down)]
    bf16 = jnp.bfloat16
    out = jax.ShapeDtypeStruct((width, NZ * 2 * LANES), bf16)
    dma = lambda n: pltpu.SemaphoreType.DMA((n,))
    vmem = lambda *shape, dtype=bf16: pltpu.VMEM(shape, dtype)
    total = EXPERTS * most
    late = 2 * (NZ - FULL)
    steps = FULL + late
    sums = [vmem(FULL, total // 2, features)] * 4 + [vmem(FULL, total // 4, features)]
    sums += [vmem(late, total // 2, LANES)] * 4 + [vmem(late, total // 4, LANES)]
    return pl.pallas_call(
        whole_kernel,
        out_shape=(out, out, out, jax.ShapeDtypeStruct((count, features), bf16)),
        in_specs=[pl.BlockSpec(memory_space=pltpu.HBM)] * 7,
        out_specs=(pl.BlockSpec(memory_space=pl.ANY),) * 3
        + (pl.BlockSpec(memory_space=pltpu.VMEM),),
        scratch_shapes=[
            vmem(NZ, width, 2 * LANES),
            vmem(NZ, width, 2 * LANES),
            vmem(2, NZ, width, LANES),
            *[pltpu.VMEM(a.shape, a.dtype) for a in (*split, gain, tokens, routes, logits)],
            vmem(2, 2, NY, rows, width),
            vmem(3, 2, NY * rows, width),
            vmem(2, width, 2 * LANES),
            vmem(2, width, LANES),
            vmem(8, count, dtype=jnp.int32),
            vmem(EXPERTS, most, features),
            vmem(2 * NX, total, features),
            vmem(total, 1, dtype=jnp.float32),
            vmem(total, width),
            *sums,
            vmem(3, total, features),
            vmem(total, features),
            vmem(EXPERTS, most, features),
            dma(3 * UNITS), dma(3 * UNITS), dma(8 * UNITS), dma(8 * UNITS),
            dma(3 * NY), dma(3 * NY), dma(2 * NX), dma(2 * NX),
            dma(steps), dma(steps), dma(2 * steps), dma(2 * steps), dma(9), dma(3 * NY), dma(3 * NY), dma(7), dma(4 * NZ),
        ],
        compiler_params=pltpu.CompilerParams(
            collective_id=0, has_side_effects=True, vmem_limit_bytes=VMEM_LIMIT
        ),
        cost_estimate=pl.CostEstimate(flops=10**11, bytes_accessed=10**7, transcendentals=0),
    )(*split, gain, tokens, routes, logits)


def shards(tokens, norm_gain, gate_train, up_train, down_train, routes, route_logits):
    *turned, mixed = whole(
        gate_train, up_train, down_train, norm_gain[None, :], tokens, routes.T, route_logits.T
    )
    return (*[w.T[None] for w in turned], mixed)


def solution(mesh):
    placed = (
        P("fs", "tp"),
        P("fs"),
        P(None, "fs", "tp"),
        P(None, "fs", "tp"),
        P(None, "fs", "tp"),
        P("fs", None),
        P("fs", None),
    )
    return jax.shard_map(
        shards,
        mesh=mesh,
        in_specs=placed,
        out_specs=(P("fs", None, "tp"), P("fs", None, "tp"), P("fs", None, "tp"), P("fs", "tp")),
        check_vma=False,
    )
```

time: 231 us -> 203 us (0.88)
  Pallas kernels: 224 us -> 192 us
  local copies, waits for them, and re-layouts: 4.39 us -> 9.03 us
    pallas_call x1, Pallas kernels: 217 us -> 192 us  [whole(): pl.pallas_call(whole_kernel, out_shape=(out, out, out, jax.ShapeDtypeStru...]
    pallas_call x1 -> x0, Pallas kernels: 7.12 us -> none  [placed_out(): pl.pallas_call(place_kernel, out_shape=(out,) * 3, in_specs=[pl.BlockSpec...]
    unnamed x6 -> x10, local copies, waits for them, and re-layouts: 2.19 us -> 9.03 us
where the time goes in v3:
time: 203 us; the launch traced here: 202 us
  Pallas kernels  192 us (95%)
  local copies, waits for them, and re-layouts  9.03 us (4%)
    pallas_call x1, Pallas kernels, whole(): pl.pallas_call(whole_kernel, out_shape=(out, out, out, jax.ShapeDtypeStru...  192 us
    unnamed x10, local copies, waits for them, and re-layouts  9.03 us

profile of v3, /device:TPU:5, one launch (start us, length us, event | category | flops | bytes accessed | tf_op | source)
XLA Modules:
  0.0 202.2 jit_solution(16727417335103970700)
XLA Ops:
  0.6 192.5 %shard_map.102 = (bf16[704,2048]{1,0:T(8,128)(2,1)}, bf16[704,2048]{1,0:T(8,128)(2,1)}, bf16[704,2048]{1,0:T(8,128)(2,1)}, bf16[384,256]{1,0:T(8,128)(2,1)}) custom-call(bf16[2,4,64,704]{3,2,1,0:T(8,128)(2,1)} %bitcast.18, bf16[2,4,64,704]{3,2,1,0:T(8,128)(2,1)} %bitcast.19, bf16[2,4,64,704]{3,2,1,0:T(8,128)(2,1)} %bitcast.20, f32[1,64]{1,0:T(1,128)} %bitcast.23, ...), custom_call_target="tpu_custom_call" | custom-call | flops 99999997952 | bytes 10000000 | tf_op jit(solution)/shard_map/pallas_call | solution.py:619
  193.1 0.0 copy-start.1
  193.1 3.9 %copy.15 = bf16[1,2048,704]{1,2,0:T(8,128)(2,1)} copy(bf16[1,2048,704]{1,2,0:T(8,128)(2,1)} %bitcast.17) | data formatting | bytes 5767168
  197.0 0.0 copy-done.1
  197.0 0.0 copy-start
  197.0 1.6 copy.16
  198.6 1.3 copy-done
  199.9 0.0 copy-start.2
  199.9 1.6 copy.17
  201.5 0.0 copy-done.2
  201.5 0.7 copy.18
Async XLA Ops:
  193.1 3.9 %copy-start.1 = (bf16[704,2048]{1,0:T(8,128)(2,1)S(1)}, bf16[704,2048]{1,0:T(8,128)(2,1)}, u32[]{:S(2)}) copy-start(bf16[704,2048]{1,0:T(8,128)(2,1)} %get-tuple-element.9) | copy-start | bytes 8650756
  197.0 2.9 %copy-start = (bf16[704,2048]{1,0:T(8,128)(2,1)S(1)}, bf16[704,2048]{1,0:T(8,128)(2,1)}, u32[]{:S(2)}) copy-start(bf16[704,2048]{1,0:T(8,128)(2,1)} %get-tuple-element.10) | copy-start | bytes 8650756
  199.9 1.6 copy-start.2

commit v4 on v3

--- a/solution.py
+++ b/solution.py
@@ -11,7 +11,7 @@
 epsilon = 1e-06
 MESH = pl.DeviceIdType.MESH
 NZ, NY = 8, 4
-VMEM_LIMIT = 60 * 1024 * 1024
+VMEM_LIMIT = 40 * 1024 * 1024
 NZ, NY, NX = 8, 4, 4
 LANES = 128
 SPLIT = ((0, 0, 128), (0, 128, 256), (0, 384, 320), (1, 0, 384), (1, 384, 320))
@@ -20,15 +20,15 @@
 UNITS = len(SPLIT) + 2
 COLS = (((1,), (0,)), ((), ()))
 ROWS = (((1,), (1,)), ((), ()))
-FULL = 5
+NEAR = 5
 
 
 def whole_kernel(
     g_in, u_in, d_in, gain_in, tok_in, route_in, logit_in,
-    g_out, u_out, d_out, mix_ref,
-    og, ou, od, g_ref, u_ref, d_ref, gain_ref, tok_ref, route_ref, logit_ref, scaled, ybuf, away, awayd, slot_ref, xs, xall, inv_ref, hidden,
-    theirs, got, mine, joint, far, theirs_h, got_h, mine_h, joint_h, far_h, parts, ret, back,
-    ysend, yrecv, zsend, zrecv, tsend, trecv, asend, arecv, psend, precv, fsend, frecv, rrecv, bsend, brecv, lsem, osem,
+    og, ou, od, mix_ref,
+    g_ref, u_ref, d_ref, gain_ref, tok_ref, route_ref, logit_ref, scaled, ybuf, away, awayd, slot_ref, xs, xall, inv_ref, hidden,
+    theirs, got, mine, joint, far, parts, ret, back,
+    ysend, yrecv, zsend, zrecv, tsend, trecv, asend, arecv, psend, precv, fsend, frecv, rrecv, bsend, brecv, lsem,
 ):
     fs = lax.axis_index("fs")
     tp = lax.axis_index("tp")
@@ -274,30 +274,30 @@
 
     def first(u):
         turn(u)
-        for kind in "ab":
+        for kind in "ba" if u >= len(SPLIT) else "ab":
             for sign in (1, -1):
                 zcopy(u, kind, sign).start()
 
-    def second(u):
-        for kind, after in (("a", "c"), ("b", "d")):
+    def second(u, kinds="ab"):
+        for kind in kinds:
             for sign in (1, -1):
                 zcopy(u, kind, sign, True).wait_recv()
-                zcopy(u, after, sign).start()
-
-    def landed(u):
-        for kind in "cd":
+                zcopy(u, {"a": "c", "b": "d"}[kind], sign).start()
+
+    def landed(u, kinds="cd"):
+        for kind in kinds:
             for sign in (1, -1):
                 zcopy(u, kind, sign, True).wait_recv()
 
     first(0)
     first(1)
     second(0)
+    first(2)
     for dz, dy in group:
         tokens_copy(dz, dy, True).wait_recv()
     for step in (1, 3, 2):
         gather_copy(step).start()
     relay_copy(0).start()
-    first(2)
     second(1)
     first(3)
     second(2)
@@ -306,12 +306,11 @@
         gather_copy(step, True).wait_recv()
         relay_copy(step).start()
     second(3)
-    first(5)
     gather_copy(2, True).wait_recv()
     relay_copy(2).start()
     second(4)
+    first(5)
     first(6)
-    second(5)
     for step in range(NX):
         relay_copy(step, True).wait_recv()
 
@@ -328,21 +327,6 @@
     lax.fori_loop(0, EXPERTS, norms, 0)
     for u in range(5):
         landed(u)
-
-    def written(m, f=0):
-        copies = []
-        for block in range(NZ):
-            if m < 2:
-                source, at, n = (og, ou)[m].at[block], block * 2 * LANES, 2 * LANES
-            else:
-                source, at, n = od.at[f, block], (block * 2 + f) * LANES, LANES
-            out = (g_out, u_out, d_out)[m].at[:, pl.ds(at, n)]
-            copies.append(pltpu.make_async_copy(source, out, osem.at[(m + f) * NZ + block]))
-        return copies
-
-    for m in range(2):
-        for copy in written(m):
-            copy.start()
 
     tile = slots // 4
 
@@ -361,7 +345,9 @@
         return carry
 
     lax.fori_loop(0, slots // tile, hide, 0)
-    second(6)
+    second(5, "b")
+    for sign in (1, -1):
+        zcopy(5, "a", sign, True).wait_recv()
 
     def block_at(k):
         return lax.rem(z + (2 * lax.rem(k, 2) - 1) * ((k + 1) // 2) + NZ, NZ)
@@ -372,57 +358,50 @@
     def quarter_rows(which, q):
         return pl.ds(pl.multiple_of(which * half_slots + q * quarter, 16), quarter)
 
-    full = (theirs, got, mine, joint, far)
-    thin = (theirs_h, got_h, mine_h, joint_h, far_h)
+    bufs = (theirs, got, mine, joint, far)
 
     def lanes(f):
-        return pl.ds(0, 2 * LANES) if f is None else pl.ds(f * LANES, LANES)
-
-    def spot(k, f):
-        if f is None:
-            return full, k, k
-        at = k - FULL + f * (NZ - FULL)
-        return thin, at, at + FULL
+        return pl.ds(f * LANES, LANES)
 
     def pair_copy(k, f):
-        bufs, at, sem = spot(k, f)
+        at = f * NZ + k
         return pltpu.make_async_remote_copy(
             src_ref=bufs[0].at[at],
             dst_ref=bufs[1].at[at],
-            send_sem=psend.at[sem],
-            recv_sem=precv.at[sem],
+            send_sem=psend.at[at],
+            recv_sem=precv.at[at],
             device_id=partner,
             device_id_type=MESH,
         )
 
     def home_copy(k, f):
-        bufs, at, sem = spot(k, f)
+        at = f * NZ + k
         return pltpu.make_async_remote_copy(
             src_ref=bufs[3].at[at],
             dst_ref=parts.at[0, half_rows(core), lanes(f)],
-            send_sem=fsend.at[sem * 2],
+            send_sem=fsend.at[at * 2],
             recv_sem=rrecv.at[8],
             device_id=partner,
             device_id_type=MESH,
         )
 
     def far_copy(k, f, q):
-        bufs, at, sem = spot(k, f)
+        at = f * NZ + k
         return pltpu.make_async_remote_copy(
             src_ref=bufs[3].at[at, pl.ds(q * quarter, quarter), :],
             dst_ref=bufs[4].at[at],
-            send_sem=fsend.at[sem * 2 + q],
-            recv_sem=frecv.at[sem * 2 + q],
+            send_sem=fsend.at[at * 2 + q],
+            recv_sem=frecv.at[at * 2 + q],
             device_id=mate(1 - 2 * q),
             device_id_type=MESH,
         )
 
     def near_copy(k, f, q, side):
-        bufs, at, sem = spot(k, f)
+        at = f * NZ + k
         return pltpu.make_async_remote_copy(
             src_ref=bufs[3].at[at, pl.ds(q * quarter, quarter), :],
             dst_ref=parts.at[1 + side, quarter_rows(core, q), lanes(f)],
-            send_sem=fsend.at[sem * 2 + q],
+            send_sem=fsend.at[at * 2 + q],
             recv_sem=rrecv.at[side * 4 + core * 2 + q],
             device_id={"tp": block_at(k)},
             device_id_type=MESH,
@@ -433,12 +412,8 @@
         return to, lax.rem(to // 2 - x + NX, NX)
 
     def project(k, f):
-        bufs, at, _ = spot(k, f)
-        block = block_at(k)
-        if f is None:
-            weights = jnp.concatenate([od[0, block], od[1, block]], axis=1)
-        else:
-            weights = od[f, block]
+        at = f * NZ + k
+        weights = od[f, block_at(k)]
         bufs[0][at] = lax.dot_general(
             hidden[half_rows(1 - core), :], weights, COLS, preferred_element_type=jnp.float32
         ).astype(jnp.bfloat16)
@@ -447,8 +422,33 @@
             hidden[half_rows(core), :], weights, COLS, preferred_element_type=jnp.float32
         ).astype(jnp.bfloat16)
 
+    def project_two(k, f):
+        at = f * NZ + k
+        weights = jnp.concatenate([od[f, block_at(k)], od[f, block_at(k + 1)]], axis=1)
+        for buf, which in ((0, 1 - core), (2, core)):
+            value = lax.dot_general(
+                hidden[half_rows(which), :], weights, COLS, preferred_element_type=jnp.float32
+            ).astype(jnp.bfloat16)
+            bufs[buf][at] = value[:, :LANES]
+            bufs[buf][at + 1] = value[:, LANES:]
+            if buf == 0:
+                pair_copy(k, f).start()
+                pair_copy(k + 1, f).start()
+
+    def project_both(k):
+        block = block_at(k)
+        weights = jnp.concatenate([od[0, block], od[1, block]], axis=1)
+        for buf, which in ((0, 1 - core), (2, core)):
+            value = lax.dot_general(
+                hidden[half_rows(which), :], weights, COLS, preferred_element_type=jnp.float32
+            ).astype(jnp.bfloat16)
+            for f in range(2):
+                bufs[buf][f * NZ + k] = value[:, f * LANES : (f + 1) * LANES]
+                if buf == 0:
+                    pair_copy(k, f).start()
+
     def join(k, f):
-        bufs, at, _ = spot(k, f)
+        at = f * NZ + k
         to, which = role(k)
         pair_copy(k, f).wait_recv()
         bufs[3][at] = (
@@ -477,7 +477,7 @@
             near_copy(k, f, 0, 1).start()
 
     def pass_on(k, f):
-        bufs, at, _ = spot(k, f)
+        at = f * NZ + k
         _, which = role(k)
         for when, q, side in ((1, 0, 0), (3, 1, 1)):
 
@@ -503,29 +503,14 @@
             far_copy(k, f, 0).wait_send()
             far_copy(k, f, 1).wait_send()
 
-    def over(what, f):
-        lo, hi = (0, FULL) if f is None else (FULL, NZ)
-
-        def step(k, carry):
-            what(k, f)
-            return carry
-
-        lax.fori_loop(lo, hi, step, 0)
-
-    over(project, None)
-    over(join, None)
-    landed(5)
-    over(project, 0)
-    over(join, 0)
-    over(pass_on, None)
-    landed(6)
-    over(project, 1)
-    for f in range(2):
-        for copy in written(2, f):
-            copy.start()
-    over(join, 1)
-    over(pass_on, 0)
-    over(pass_on, 1)
+    def near(f):
+        project_two(0, f)
+        project_two(2, f)
+        join(0, f)
+        join(1, f)
+        project(4, f)
+        for k in (2, 3, 4):
+            join(k, f)
 
     def whole_wait(place, sem):
         pltpu.make_async_remote_copy(
@@ -537,23 +522,67 @@
             device_id_type=MESH,
         ).wait_recv()
 
-    whole_wait(parts.at[0, half_rows(1 - core), :], 8)
-    for side in range(2):
-        for c in range(2):
-            for q in range(2):
-                whole_wait(parts.at[1 + side, quarter_rows(c, q), :], side * 4 + c * 2 + q)
-
-    def total(at):
+    def total(c, q):
+        at = quarter_rows(c, q)
         value = parts[0, at, :].astype(jnp.float32)
-        for block in range(1, 3):
-            value = value + parts[block, at, :].astype(jnp.float32)
+        for side in range(2):
+            whole_wait(parts.at[1 + side, at, :], side * 4 + c * 2 + q)
+            value = value + parts[1 + side, at, :].astype(jnp.float32)
         ret[at, :] = value.astype(jnp.bfloat16)
 
-    for dz, dy in group:
-        total(arrived_rows(dz, yat(dy)))
-        back_copy(dz, dy).start()
-    total(arrived_rows(0, y))
-    back[here] = ret[arrived_rows(0, y), :]
+    def give_back():
+        whole_wait(parts.at[0, half_rows(1 - core), :], 8)
+        for q, dz in ((0, 1), (1, -1)):
+            total(1, q)
+            for dy in (0, 1, 3, 2):
+                back_copy(dz, dy).start()
+        total(0, 0)
+        total(0, 1)
+        for dy in (1, 3, 2):
+            back_copy(0, dy).start()
+        back[here] = ret[arrived_rows(0, y), :]
+
+    away_by = lax.rem(tp - z + NZ, NZ)
+    early = (away_by <= 2) | (away_by >= 6)
+
+    near(0)
+    second(6, "b")
+    for sign in (1, -1):
+        zcopy(5, "c", sign).start()
+    second(6, "a")
+    near(1)
+    for k in range(NEAR):
+        pass_on(k, 0)
+    landed(5, "d")
+    landed(6, "d")
+    project_both(NZ - 1)
+    for f in range(2):
+        join(NZ - 1, f)
+    for k in range(NEAR):
+        pass_on(k, 1)
+    landed(5, "c")
+    project_two(NEAR, 0)
+    for f in range(2):
+        pass_on(NZ - 1, f)
+    for k in (NEAR, NEAR + 1):
+        join(k, 0)
+
+    @pl.when(early)
+    def _():
+        give_back()
+
+    landed(6, "c")
+    project_two(NEAR, 1)
+    for k in (NEAR, NEAR + 1):
+        join(k, 1)
+    for f in range(2):
+        for k in (NEAR, NEAR + 1):
+            pass_on(k, f)
+
+    @pl.when(jnp.logical_not(early))
+    def _():
+        give_back()
+
     for dz, dy in group:
         back_copy(dz, dy, True).wait_recv()
 
@@ -595,11 +624,8 @@
         gather_copy(step).wait_send()
     for step in range(NX):
         relay_copy(step).wait_send()
-    for f in (None, 0, 1):
-        over(sent, f)
-    for m, f in ((0, 0), (1, 0), (2, 0), (2, 1)):
-        for copy in written(m, f):
-            copy.wait()
+    for f in range(2):
+        lax.fori_loop(0, NZ, lambda k, carry: (sent(k, f), carry)[1], 0)
 
 
 def whole(gate, up, down, gain, tokens, routes, logits):
@@ -607,26 +633,26 @@
     count, features = tokens.shape
     most = count // 2
     split = [w.reshape(2, NY, rows, width) for w in (gate, up, down)]
+    given = (*split, gain, tokens, routes, logits)
     bf16 = jnp.bfloat16
-    out = jax.ShapeDtypeStruct((width, NZ * 2 * LANES), bf16)
+    out = jax.ShapeDtypeStruct((NZ, width, 2 * LANES), bf16)
     dma = lambda n: pltpu.SemaphoreType.DMA((n,))
     vmem = lambda *shape, dtype=bf16: pltpu.VMEM(shape, dtype)
     total = EXPERTS * most
-    late = 2 * (NZ - FULL)
-    steps = FULL + late
-    sums = [vmem(FULL, total // 2, features)] * 4 + [vmem(FULL, total // 4, features)]
-    sums += [vmem(late, total // 2, LANES)] * 4 + [vmem(late, total // 4, LANES)]
+    steps = 2 * NZ
+    sums = [vmem(steps, total // 2, LANES)] * 4 + [vmem(steps, total // 4, LANES)]
     return pl.pallas_call(
         whole_kernel,
-        out_shape=(out, out, out, jax.ShapeDtypeStruct((count, features), bf16)),
+        out_shape=(
+            out,
+            out,
+            jax.ShapeDtypeStruct((2, NZ, width, LANES), bf16),
+            jax.ShapeDtypeStruct((count, features), bf16),
+        ),
         in_specs=[pl.BlockSpec(memory_space=pltpu.HBM)] * 7,
-        out_specs=(pl.BlockSpec(memory_space=pl.ANY),) * 3
-        + (pl.BlockSpec(memory_space=pltpu.VMEM),),
+        out_specs=(pl.BlockSpec(memory_space=pltpu.VMEM),) * 4,
         scratch_shapes=[
-            vmem(NZ, width, 2 * LANES),
-            vmem(NZ, width, 2 * LANES),
-            vmem(2, NZ, width, LANES),
-            *[pltpu.VMEM(a.shape, a.dtype) for a in (*split, gain, tokens, routes, logits)],
+            *[pltpu.VMEM(a.shape, a.dtype) for a in given],
             vmem(2, 2, NY, rows, width),
             vmem(3, 2, NY * rows, width),
             vmem(2, width, 2 * LANES),
@@ -642,20 +668,54 @@
             vmem(EXPERTS, most, features),
             dma(3 * UNITS), dma(3 * UNITS), dma(8 * UNITS), dma(8 * UNITS),
             dma(3 * NY), dma(3 * NY), dma(2 * NX), dma(2 * NX),
-            dma(steps), dma(steps), dma(2 * steps), dma(2 * steps), dma(9), dma(3 * NY), dma(3 * NY), dma(7), dma(4 * NZ),
+            dma(steps), dma(steps), dma(2 * steps), dma(2 * steps), dma(9), dma(3 * NY), dma(3 * NY), dma(7),
         ],
         compiler_params=pltpu.CompilerParams(
             collective_id=0, has_side_effects=True, vmem_limit_bytes=VMEM_LIMIT
         ),
         cost_estimate=pl.CostEstimate(flops=10**11, bytes_accessed=10**7, transcendentals=0),
-    )(*split, gain, tokens, routes, logits)
+    )(*[pltpu.with_memory_space_constraint(a, pltpu.HBM) for a in given])
+
+
+def place_kernel(g_ref, u_ref, d_ref, m_ref, og, ou, od, om, sem):
+    copies = [pltpu.make_async_copy(m_ref, om, sem.at[4 * NZ])]
+    for m, (ref, out) in enumerate(((g_ref, og), (u_ref, ou))):
+        for block in range(NZ):
+            columns = pl.ds(block * 2 * LANES, 2 * LANES)
+            copies.append(
+                pltpu.make_async_copy(ref.at[block], out.at[:, columns], sem.at[m * NZ + block])
+            )
+    for f in range(2):
+        for block in range(NZ):
+            columns = pl.ds((block * 2 + f) * LANES, LANES)
+            at = (2 + f) * NZ + block
+            copies.append(pltpu.make_async_copy(d_ref.at[f, block], od.at[:, columns], sem.at[at]))
+    for copy in copies:
+        copy.start()
+    for copy in copies:
+        copy.wait()
+
+
+def placed_out(blocks):
+    nz, width, size = blocks[0].shape
+    out = jax.ShapeDtypeStruct((width, nz * size), jnp.bfloat16)
+    *turned, mixed = pl.pallas_call(
+        place_kernel,
+        out_shape=(out, out, out, jax.ShapeDtypeStruct(blocks[3].shape, jnp.bfloat16)),
+        in_specs=[pl.BlockSpec(memory_space=pltpu.VMEM)] * 4,
+        out_specs=(pl.BlockSpec(memory_space=pl.ANY),) * 4,
+        scratch_shapes=[pltpu.SemaphoreType.DMA((4 * NZ + 1,))],
+        compiler_params=pltpu.CompilerParams(vmem_limit_bytes=2 * 1024 * 1024),
+    )(*blocks)
+    return (*[w.T[None] for w in turned], mixed)
 
 
 def shards(tokens, norm_gain, gate_train, up_train, down_train, routes, route_logits):
-    *turned, mixed = whole(
-        gate_train, up_train, down_train, norm_gain[None, :], tokens, routes.T, route_logits.T
+    return placed_out(
+        whole(
+            gate_train, up_train, down_train, norm_gain[None, :], tokens, routes.T, route_logits.T
+        )
     )
-    return (*[w.T[None] for w in turned], mixed)
 
 
 def solution(mesh):

time: 203 us -> 189 us (0.931)
  local copies, waits for them, and re-layouts: 9.03 us -> 0 us
  Pallas kernels: 192 us -> 188 us
    unnamed x10 -> x0, local copies, waits for them, and re-layouts: 9.03 us -> none
    pallas_call x1 -> x2, Pallas kernels: 192 us -> 188 us  [the longest x1 184 us: whole(): pl.pallas_call(whole_kernel, out_shape=(out, out, jax.ShapeDtypeStruct((2...]
where the time goes in v4:
time: 189 us
  Pallas kernels  188 us (99%)
    pallas_call x1, Pallas kernels, whole(): pl.pallas_call(whole_kernel, out_shape=(out, out, jax.ShapeDtypeStruct((2...  184 us

profile of v4, /device:TPU:5, one launch (start us, length us, event | category | flops | bytes accessed | tf_op | source)
XLA Modules:
  0.0 188.6 jit_solution(9418510242998601755)
XLA Ops:
  0.6 184.1 %shard_map.102 = (bf16[8,704,256]{2,1,0:T(8,128)(2,1)S(1)}, bf16[8,704,256]{2,1,0:T(8,128)(2,1)S(1)}, bf16[2,8,704,128]{3,2,1,0:T(8,128)(2,1)S(1)}, bf16[384,256]{1,0:T(8,128)(2,1)S(1)}) custom-call(bf16[2,4,64,704]{3,2,1,0:T(8,128)(2,1)} %bitcast.18, bf16[2,4,64,704]{3,2,1,0:T(8,128)(2,1)} %bitcast.19, bf16[2,4,64,704]{3,2,1,0:T(8,128)(2,1)} %bitcast.20, ...), custom_call_target="tpu_custom_call" | custom-call | flops 99999997952 | bytes 10000000 | tf_op jit(solution)/shard_map/pallas_call | solution.py:644
  184.7 3.7 %shard_map.103 = (bf16[704,2048]{1,0:T(8,128)(2,1)}, bf16[704,2048]{1,0:T(8,128)(2,1)}, bf16[704,2048]{1,0:T(8,128)(2,1)}, bf16[384,256]{1,0:T(8,128)(2,1)}) custom-call(bf16[8,704,256]{2,1,0:T(8,128)(2,1)S(1)} %get-tuple-element.12.g_ref, bf16[8,704,256]{2,1,0:T(8,128)(2,1)S(1)} %get-tuple-element.13.u_ref, ...), custom_call_target="tpu_custom_call" | custom-call | tf_op jit(solution)/shard_map/pallas_call | solution.py:702

commit v5 on v4

--- a/solution.py
+++ b/solution.py
@@ -145,12 +145,15 @@
             device_id_type=MESH,
         )
 
-    def back_copy(dz, dy, arriving=False):
-        at = (dz + 1) * NY + dy
+    def lanes(f):
+        return pl.ds(f * LANES, LANES)
+
+    def back_copy(dz, dy, f, arriving=False):
+        at = (f * 3 + dz + 1) * NY + dy
         owner = expert(dz, yat(-dy)) if arriving else here
         return pltpu.make_async_remote_copy(
-            src_ref=ret.at[arrived_rows(dz, yat(dy)), :],
-            dst_ref=back.at[owner, held_rows(dz), :],
+            src_ref=ret.at[arrived_rows(dz, yat(dy)), lanes(f)],
+            dst_ref=back.at[owner, held_rows(dz), lanes(f)],
             send_sem=bsend.at[at],
             recv_sem=brecv.at[at],
             device_id=device(-dz, dy),
@@ -272,9 +275,10 @@
                     awayd[f, pl.ds(lo, n), :] = gone[:, f * LANES : (f + 1) * LANES]
                     od[f, z, pl.ds(lo, n), :] = kept[:, f * LANES : (f + 1) * LANES]
 
-    def first(u):
-        turn(u)
-        for kind in "ba" if u >= len(SPLIT) else "ab":
+    def first(u, kinds=None):
+        if kinds != "a":
+            turn(u)
+        for kind in kinds or ("ba" if u >= len(SPLIT) else "ab"):
             for sign in (1, -1):
                 zcopy(u, kind, sign).start()
 
@@ -310,7 +314,7 @@
     relay_copy(2).start()
     second(4)
     first(5)
-    first(6)
+    first(6, "b")
     for step in range(NX):
         relay_copy(step, True).wait_recv()
 
@@ -345,9 +349,8 @@
         return carry
 
     lax.fori_loop(0, slots // tile, hide, 0)
-    second(5, "b")
-    for sign in (1, -1):
-        zcopy(5, "a", sign, True).wait_recv()
+    second(5, "ba")
+    first(6, "a")
 
     def block_at(k):
         return lax.rem(z + (2 * lax.rem(k, 2) - 1) * ((k + 1) // 2) + NZ, NZ)
@@ -359,9 +362,6 @@
         return pl.ds(pl.multiple_of(which * half_slots + q * quarter, 16), quarter)
 
     bufs = (theirs, got, mine, joint, far)
-
-    def lanes(f):
-        return pl.ds(f * LANES, LANES)
 
     def pair_copy(k, f):
         at = f * NZ + k
@@ -380,7 +380,7 @@
             src_ref=bufs[3].at[at],
             dst_ref=parts.at[0, half_rows(core), lanes(f)],
             send_sem=fsend.at[at * 2],
-            recv_sem=rrecv.at[8],
+            recv_sem=rrecv.at[f * 9 + 8],
             device_id=partner,
             device_id_type=MESH,
         )
@@ -402,7 +402,7 @@
             src_ref=bufs[3].at[at, pl.ds(q * quarter, quarter), :],
             dst_ref=parts.at[1 + side, quarter_rows(core, q), lanes(f)],
             send_sem=fsend.at[at * 2 + q],
-            recv_sem=rrecv.at[side * 4 + core * 2 + q],
+            recv_sem=rrecv.at[f * 9 + side * 4 + core * 2 + q],
             device_id={"tp": block_at(k)},
             device_id_type=MESH,
         )
@@ -522,69 +522,59 @@
             device_id_type=MESH,
         ).wait_recv()
 
-    def total(c, q):
+    def total(c, q, f):
         at = quarter_rows(c, q)
-        value = parts[0, at, :].astype(jnp.float32)
+        value = parts[0, at, lanes(f)].astype(jnp.float32)
         for side in range(2):
-            whole_wait(parts.at[1 + side, at, :], side * 4 + c * 2 + q)
-            value = value + parts[1 + side, at, :].astype(jnp.float32)
-        ret[at, :] = value.astype(jnp.bfloat16)
-
-    def give_back():
-        whole_wait(parts.at[0, half_rows(1 - core), :], 8)
+            whole_wait(parts.at[1 + side, at, lanes(f)], f * 9 + side * 4 + c * 2 + q)
+            value = value + parts[1 + side, at, lanes(f)].astype(jnp.float32)
+        ret[at, lanes(f)] = value.astype(jnp.bfloat16)
+
+    def give_back(f):
+        whole_wait(parts.at[0, half_rows(1 - core), lanes(f)], f * 9 + 8)
         for q, dz in ((0, 1), (1, -1)):
-            total(1, q)
+            total(1, q, f)
             for dy in (0, 1, 3, 2):
-                back_copy(dz, dy).start()
-        total(0, 0)
-        total(0, 1)
+                back_copy(dz, dy, f).start()
+        total(0, 0, f)
+        total(0, 1, f)
         for dy in (1, 3, 2):
-            back_copy(0, dy).start()
-        back[here] = ret[arrived_rows(0, y), :]
-
-    away_by = lax.rem(tp - z + NZ, NZ)
-    early = (away_by <= 2) | (away_by >= 6)
-
+            back_copy(0, dy, f).start()
+        back[here, :, lanes(f)] = ret[arrived_rows(0, y), lanes(f)]
+
+    def each(what, ks, f):
+        for k in ks:
+            what(k, f)
+
+    close = range(NEAR)
+    final = (NEAR, NEAR + 1)
     near(0)
     second(6, "b")
-    for sign in (1, -1):
-        zcopy(5, "c", sign).start()
+    landed(5, "d")
+    project(NZ - 1, 0)
+    join(NZ - 1, 0)
+    each(pass_on, close, 0)
+    landed(5, "c")
+    project_two(NEAR, 0)
+    each(join, final, 0)
     second(6, "a")
     near(1)
-    for k in range(NEAR):
-        pass_on(k, 0)
-    landed(5, "d")
+    each(pass_on, (NZ - 1, NEAR, NEAR + 1), 0)
     landed(6, "d")
-    project_both(NZ - 1)
-    for f in range(2):
-        join(NZ - 1, f)
-    for k in range(NEAR):
-        pass_on(k, 1)
-    landed(5, "c")
-    project_two(NEAR, 0)
-    for f in range(2):
-        pass_on(NZ - 1, f)
-    for k in (NEAR, NEAR + 1):
-        join(k, 0)
-
-    @pl.when(early)
-    def _():
-        give_back()
-
+    project(NZ - 1, 1)
+    join(NZ - 1, 1)
     landed(6, "c")
     project_two(NEAR, 1)
-    for k in (NEAR, NEAR + 1):
-        join(k, 1)
+    each(join, final, 1)
+    each(pass_on, close, 1)
+    pass_on(NZ - 1, 1)
+    give_back(0)
+    each(pass_on, final, 1)
+    give_back(1)
+
     for f in range(2):
-        for k in (NEAR, NEAR + 1):
-            pass_on(k, f)
-
-    @pl.when(jnp.logical_not(early))
-    def _():
-        give_back()
-
-    for dz, dy in group:
-        back_copy(dz, dy, True).wait_recv()
+        for dz, dy in group:
+            back_copy(dz, dy, f, True).wait_recv()
 
     count = tok_ref.shape[0]
     piece = count // 3
@@ -619,7 +609,8 @@
                 zcopy(u, kind, sign).wait_send()
     for dz, dy in group:
         tokens_copy(dz, dy).wait_send()
-        back_copy(dz, dy).wait_send()
+        for f in range(2):
+            back_copy(dz, dy, f).wait_send()
     for step in range(1, NX):
         gather_copy(step).wait_send()
     for step in range(NX):
@@ -668,7 +659,7 @@
             vmem(EXPERTS, most, features),
             dma(3 * UNITS), dma(3 * UNITS), dma(8 * UNITS), dma(8 * UNITS),
             dma(3 * NY), dma(3 * NY), dma(2 * NX), dma(2 * NX),
-            dma(steps), dma(steps), dma(2 * steps), dma(2 * steps), dma(9), dma(3 * NY), dma(3 * NY), dma(7),
+            dma(steps), dma(steps), dma(2 * steps), dma(2 * steps), dma(18), dma(6 * NY), dma(6 * NY), dma(7),
         ],
         compiler_params=pltpu.CompilerParams(
             collective_id=0, has_side_effects=True, vmem_limit_bytes=VMEM_LIMIT

time: 189 us -> 185 us (0.979)
  Pallas kernels: 188 us -> 184 us
    pallas_call x1, Pallas kernels: 184 us -> 180 us  [whole(): pl.pallas_call(whole_kernel, out_shape=(out, out, jax.ShapeDtypeStruct((2...]
where the time goes in v5:
time: 185 us
  Pallas kernels  184 us (99%)
    pallas_call x1, Pallas kernels, whole(): pl.pallas_call(whole_kernel, out_shape=(out, out, jax.ShapeDtypeStruct((2...  180 us

profile of v5, /device:TPU:5, one launch (start us, length us, event | category | flops | bytes accessed | tf_op | source)
XLA Modules:
  0.0 184.5 jit_solution(5310193120859646034)
XLA Ops:
  0.6 180.0 %shard_map.102 = (bf16[8,704,256]{2,1,0:T(8,128)(2,1)S(1)}, bf16[8,704,256]{2,1,0:T(8,128)(2,1)S(1)}, bf16[2,8,704,128]{3,2,1,0:T(8,128)(2,1)S(1)}, bf16[384,256]{1,0:T(8,128)(2,1)S(1)}) custom-call(bf16[2,4,64,704]{3,2,1,0:T(8,128)(2,1)} %bitcast.18, bf16[2,4,64,704]{3,2,1,0:T(8,128)(2,1)} %bitcast.19, bf16[2,4,64,704]{3,2,1,0:T(8,128)(2,1)} %bitcast.20, ...), custom_call_target="tpu_custom_call" | custom-call | flops 99999997952 | bytes 10000000 | tf_op jit(solution)/shard_map/pallas_call | solution.py:635
  180.7 3.7 %shard_map.103 = (bf16[704,2048]{1,0:T(8,128)(2,1)}, bf16[704,2048]{1,0:T(8,128)(2,1)}, bf16[704,2048]{1,0:T(8,128)(2,1)}, bf16[384,256]{1,0:T(8,128)(2,1)}) custom-call(bf16[8,704,256]{2,1,0:T(8,128)(2,1)S(1)} %get-tuple-element.12.g_ref, bf16[8,704,256]{2,1,0:T(8,128)(2,1)S(1)} %get-tuple-element.13.u_ref, ...), custom_call_target="tpu_custom_call" | custom-call | tf_op jit(solution)/shard_map/pallas_call | solution.py:693

commit v6 on v5

--- a/solution.py
+++ b/solution.py
@@ -27,7 +27,7 @@
     g_in, u_in, d_in, gain_in, tok_in, route_in, logit_in,
     og, ou, od, mix_ref,
     g_ref, u_ref, d_ref, gain_ref, tok_ref, route_ref, logit_ref, scaled, ybuf, away, awayd, slot_ref, xs, xall, inv_ref, hidden,
-    theirs, got, mine, joint, far, parts, ret, back,
+    theirs, got, mine, joint, far, parts, ret, back, chosen_ref, share_ref,
     ysend, yrecv, zsend, zrecv, tsend, trecv, asend, arecv, psend, precv, fsend, frecv, rrecv, bsend, brecv, lsem,
 ):
     fs = lax.axis_index("fs")
@@ -81,7 +81,6 @@
     greeted += [{"tp": lax.rem(tp + step, 2 * NX)} for step in range(1, 2 * NX)]
     for other in greeted:
         pl.semaphore_signal(barrier, inc=1, device_id=other, device_id_type=MESH)
-    pl.semaphore_wait(barrier, len(greeted))
 
     def ycopy(u, dy, to_row):
         m, lo, n = ACROSS[u]
@@ -236,6 +235,7 @@
     for load in loads[:2]:
         load.wait()
     scale(0, g_ref)
+    pl.semaphore_wait(barrier, len(greeted))
     across(0)
     for load in loads[2:]:
         load.wait()
@@ -329,6 +329,28 @@
         return carry
 
     lax.fori_loop(0, EXPERTS, norms, 0)
+
+    count = tok_ref.shape[0]
+    piece = count // 3
+
+    def choose(i, carry):
+        at = pl.ds(pl.multiple_of(i * piece, 16), piece)
+        ids = lax.broadcasted_iota(jnp.int32, (piece, slots), 1)
+        on = lax.broadcasted_iota(jnp.int32, (piece, count), 1) == (
+            lax.broadcasted_iota(jnp.int32, (piece, count), 0) + i * piece
+        )
+
+        def column(line):
+            return jnp.sum(jnp.where(on, line, 0.0), axis=1, keepdims=True)
+
+        scores = [column(logit_ref[k : k + 1, :]) for k in range(2)]
+        for k in range(2):
+            wanted = column(slot_ref[k : k + 1, :].astype(jnp.float32)).astype(jnp.int32)
+            chosen_ref[k, at, :] = jnp.where(ids == wanted, 1.0, 0.0).astype(jnp.bfloat16)
+            share_ref[at, k : k + 1] = jax.nn.sigmoid(scores[k] - scores[1 - k])
+        return carry
+
+    lax.fori_loop(0, count // piece, choose, 0)
     for u in range(5):
         landed(u)
 
@@ -572,34 +594,25 @@
     each(pass_on, final, 1)
     give_back(1)
 
+    def mix(f):
+        def one(i, carry):
+            at = pl.ds(pl.multiple_of(i * piece, 16), piece)
+            results = back[:, :, lanes(f)].reshape(slots, LANES)
+            value = jnp.zeros((piece, LANES), jnp.float32)
+            for k in range(2):
+                picked = jnp.dot(
+                    chosen_ref[k, at, :], results, preferred_element_type=jnp.float32
+                )
+                value = value + picked * share_ref[at, k : k + 1]
+            mix_ref[at, lanes(f)] = value.astype(jnp.bfloat16)
+            return carry
+
+        lax.fori_loop(0, count // piece, one, 0)
+
     for f in range(2):
         for dz, dy in group:
             back_copy(dz, dy, f, True).wait_recv()
-
-    count = tok_ref.shape[0]
-    piece = count // 3
-
-    def mix(i, carry):
-        ids = lax.broadcasted_iota(jnp.int32, (piece, slots), 1)
-        on = lax.broadcasted_iota(jnp.int32, (piece, count), 1) == (
-            lax.broadcasted_iota(jnp.int32, (piece, count), 0) + i * piece
-        )
-
-        def column(line):
-            return jnp.sum(jnp.where(on, line, 0.0), axis=1, keepdims=True)
-
-        results = back[...].reshape(slots, back.shape[2])
-        scores = [column(logit_ref[k : k + 1, :]) for k in range(2)]
-        value = jnp.zeros((piece, back.shape[2]), jnp.float32)
-        for k in range(2):
-            wanted = column(slot_ref[k : k + 1, :].astype(jnp.float32)).astype(jnp.int32)
-            chosen = jnp.where(ids == wanted, 1.0, 0.0).astype(jnp.bfloat16)
-            picked = jnp.dot(chosen, results, preferred_element_type=jnp.float32)
-            value = value + picked * jax.nn.sigmoid(scores[k] - scores[1 - k])
-        mix_ref[pl.ds(pl.multiple_of(i * piece, 16), piece), :] = value.astype(jnp.bfloat16)
-        return carry
-
-    lax.fori_loop(0, count // piece, mix, 0)
+        mix(f)
 
     for u in range(UNITS):
         for dy in (1, 3, 2):
@@ -657,6 +670,8 @@
             vmem(3, total, features),
             vmem(total, features),
             vmem(EXPERTS, most, features),
+            vmem(2, count, total),
+            vmem(count, LANES, dtype=jnp.float32),
             dma(3 * UNITS), dma(3 * UNITS), dma(8 * UNITS), dma(8 * UNITS),
             dma(3 * NY), dma(3 * NY), dma(2 * NX), dma(2 * NX),
             dma(steps), dma(steps), dma(2 * steps), dma(2 * steps), dma(18), dma(6 * NY), dma(6 * NY), dma(7),

time: 185 us -> 184 us (level)
  no operation moved by 1% of the time
where the time goes in v6:
time: 184 us
  Pallas kernels  183 us (99%)
    pallas_call x1, Pallas kernels, whole(): pl.pallas_call(whole_kernel, out_shape=(out, out, jax.ShapeDtypeStruct((2...  179 us
    pallas_call x1, Pallas kernels, placed_out(): pl.pallas_call(place_kernel, out_shape=(out, out, out, jax.ShapeDtypeStru...  3.69 us

profile of v6, /device:TPU:5, one launch (start us, length us, event | category | flops | bytes accessed | tf_op | source)
XLA Modules:
  0.0 184.0 jit_solution(17113960302967573236)
XLA Ops:
  0.6 179.5 %shard_map.102 = (bf16[8,704,256]{2,1,0:T(8,128)(2,1)S(1)}, bf16[8,704,256]{2,1,0:T(8,128)(2,1)S(1)}, bf16[2,8,704,128]{3,2,1,0:T(8,128)(2,1)S(1)}, bf16[384,256]{1,0:T(8,128)(2,1)S(1)}) custom-call(bf16[2,4,64,704]{3,2,1,0:T(8,128)(2,1)} %bitcast.18, bf16[2,4,64,704]{3,2,1,0:T(8,128)(2,1)} %bitcast.19, bf16[2,4,64,704]{3,2,1,0:T(8,128)(2,1)} %bitcast.20, ...), custom_call_target="tpu_custom_call" | custom-call | flops 99999997952 | bytes 10000000 | tf_op jit(solution)/shard_map/pallas_call | solution.py:648
  180.1 3.7 %shard_map.103 = (bf16[704,2048]{1,0:T(8,128)(2,1)}, bf16[704,2048]{1,0:T(8,128)(2,1)}, bf16[704,2048]{1,0:T(8,128)(2,1)}, bf16[384,256]{1,0:T(8,128)(2,1)}) custom-call(bf16[8,704,256]{2,1,0:T(8,128)(2,1)S(1)} %get-tuple-element.12.g_ref, bf16[8,704,256]{2,1,0:T(8,128)(2,1)S(1)} %get-tuple-element.13.u_ref, ...), custom_call_target="tpu_custom_call" | custom-call | tf_op jit(solution)/shard_map/pallas_call | solution.py:708

commit v7 on v6

--- a/solution.py
+++ b/solution.py
@@ -14,7 +14,7 @@
 VMEM_LIMIT = 40 * 1024 * 1024
 NZ, NY, NX = 8, 4, 4
 LANES = 128
-SPLIT = ((0, 0, 128), (0, 128, 256), (0, 384, 320), (1, 0, 384), (1, 384, 320))
+SPLIT = ((0, 0, 128), (0, 128, 128), (0, 256, 448), (1, 0, 384), (1, 384, 320))
 DOWN = ((2, 0, 384), (2, 384, 320))
 ACROSS = SPLIT + DOWN
 UNITS = len(SPLIT) + 2

time: 184 us -> 185 us (level)
  no operation moved by 1% of the time
where the time goes in v7:
time: 185 us; the launch traced here: 183 us
  Pallas kernels  182 us (98%)
    pallas_call x1, Pallas kernels, whole(): pl.pallas_call(whole_kernel, out_shape=(out, out, jax.ShapeDtypeStruct((2...  179 us

profile of v7, /device:TPU:5, one launch (start us, length us, event | category | flops | bytes accessed | tf_op | source)
XLA Modules:
  0.0 183.3 jit_solution(17539937465520975811)
XLA Ops:
  0.6 178.8 %shard_map.102 = (bf16[8,704,256]{2,1,0:T(8,128)(2,1)S(1)}, bf16[8,704,256]{2,1,0:T(8,128)(2,1)S(1)}, bf16[2,8,704,128]{3,2,1,0:T(8,128)(2,1)S(1)}, bf16[384,256]{1,0:T(8,128)(2,1)S(1)}) custom-call(bf16[2,4,64,704]{3,2,1,0:T(8,128)(2,1)} %bitcast.18, bf16[2,4,64,704]{3,2,1,0:T(8,128)(2,1)} %bitcast.19, bf16[2,4,64,704]{3,2,1,0:T(8,128)(2,1)} %bitcast.20, ...), custom_call_target="tpu_custom_call" | custom-call | flops 99999997952 | bytes 10000000 | tf_op jit(solution)/shard_map/pallas_call | solution.py:648
  179.4 3.7 %shard_map.103 = (bf16[704,2048]{1,0:T(8,128)(2,1)}, bf16[704,2048]{1,0:T(8,128)(2,1)}, bf16[704,2048]{1,0:T(8,128)(2,1)}, bf16[384,256]{1,0:T(8,128)(2,1)}) custom-call(bf16[8,704,256]{2,1,0:T(8,128)(2,1)S(1)} %get-tuple-element.12.g_ref, bf16[8,704,256]{2,1,0:T(8,128)(2,1)S(1)} %get-tuple-element.13.u_ref, ...), custom_call_target="tpu_custom_call" | custom-call | tf_op jit(solution)/shard_map/pallas_call | solution.py:708
